TPU v7x, 256 devices: a 4x2x16 block of a 4x16x16 slice. The times are simulated.
256 devices in a mesh: grp: 2 (over y), sp: 16 (over z), tp: 8 (over x, core).
Axes of the slice: x: 4, y: 2, z: 16, core: 2. Of those that a mesh axis runs over, the one named last changes fastest.
The devices are a block of a 4x16x16 slice.
Arguments:
- hidden_in: bfloat16 [12288, 4096], P(('grp', 'sp'), 'tp'), parts along dimension 0, may hold values from -30 to 30
- in_gain: float32 [2, 4096], P(None, 'tp'), may hold values from 0.1 to 1.9
- w_value: bfloat16 [2, 4096, 2048], P(None, 'sp', 'tp'), may hold values from -0.09375 to 0.09375
- w_gate: bfloat16 [2, 4096, 2048], P(None, 'sp', 'tp'), may hold values from -0.09375 to 0.09375
- conv_taps: float32 [2, 31, 2048], P(None, None, 'tp'), may hold values from -9 to 9
- norm_gain: float32 [2, 2048], P(None, 'tp'), may hold values from 0.1 to 1.9
- norm_shift: float32 [2, 2048], P(None, 'tp'), may hold values from -3 to 3
- w_out: bfloat16 [2, 2048, 4096], P(None, 'tp', 'sp'), may hold values from -0.125 to 0.125
Outputs:
- hidden_out: bfloat16 [12288, 4096], P(('grp', 'sp'), 'tp'), parts along dimension 0
There are 2 independent parts, one for each index of `grp`. A program takes and returns all parts, laid end to end along the dimension named above; an argument that names none is the same for every part. Nothing has to cross between parts.
All inputs are finite; a program needn't handle non-finite values.
Results may differ from a plain program's by a relative error of at most 0.013.
Values may be sent and summed in bfloat16 or wider, within the bound.
A program may use at most 64 MiB of HBM per device.

v0:
```python
import jax
import jax.numpy as jnp
from jax import lax
from jax.sharding import PartitionSpec as P

D = 4096
C = 2048


epsilon = 1e-06


def from_everyone(x, axis):
    size = lax.axis_size(axis)
    return lax.all_to_all(jnp.broadcast_to(x[None], (size, *x.shape)), axis, 0, 0, tiled=True)


def taken_together(x, axis):
    return from_everyone(x, axis).sum(axis=0)


def laid_out(parts, dim):
    parts = jnp.moveaxis(parts, 0, dim)
    shape = parts.shape
    return parts.reshape(*shape[:dim], shape[dim] * shape[dim + 1], *shape[dim + 2 :])


def gathered_copies(x, axis, dim):
    parts = from_everyone(x, axis)
    return laid_out(parts, dim)


def side_by_side(arrays, axis, dim, along):
    ends, at = ([], 0)
    for a in arrays[:-1]:
        at += a.shape[along]
        ends.append(at)
    both = jnp.concatenate(arrays, axis=along)
    return tuple(jnp.split(lax.all_gather(both, axis, axis=dim, tiled=True), ends, axis=along))


def passed_along(value, axis, steps):
    count = lax.axis_size(axis)
    initial, last = (max(0, -steps), min(count, count - steps))
    return lax.ppermute(value, axis, [(source, source + steps) for source in range(initial, last)])


def depthwise(extended, kernel_taps):
    conved = lax.conv_general_dilated(
        extended.astype(jnp.float32)[None],
        kernel_taps[:, None, :],
        (1,),
        [(0, 0)],
        dimension_numbers=("NWC", "WIO", "NWC"),
        feature_group_count=extended.shape[1],
        precision=lax.Precision.HIGHEST,
    )
    return conved[0]


def shards(hidden_in, in_gain, w_value, w_gate, conv_taps, norm_gain, norm_shift, w_out):
    layer_count = w_value.shape[0]
    reach_rows = conv_taps.shape[1] - 1
    current = hidden_in
    for layer_idx in range(layer_count):
        widened = current.astype(jnp.float32)
        squares = taken_together(jnp.sum(widened * widened, axis=1), "tp")
        normalized = (
            widened * lax.rsqrt(squares / D + epsilon)[:, None] * in_gain[layer_idx]
        ).astype(jnp.bfloat16)
        gathered = gathered_copies(normalized, "tp", 1)
        zero_init = jnp.zeros((gathered.shape[0], w_value.shape[2]), jnp.float32)
        pieces = side_by_side((w_value[layer_idx], w_gate[layer_idx]), "sp", 0, 1)
        columns = lax.slice_in_dim(gathered, 0, pieces[0].shape[0], axis=1)
        value_part = zero_init + jnp.dot(columns, pieces[0], preferred_element_type=jnp.float32)
        gate_part = zero_init + jnp.dot(columns, pieces[1], preferred_element_type=jnp.float32)
        gated = (value_part * jax.nn.sigmoid(gate_part)).astype(jnp.bfloat16)
        before = passed_along(gated[gated.shape[0] - reach_rows :], "sp", 1)
        extended = jnp.concatenate([before, gated], axis=0)
        residual = current
        conved = depthwise(extended, conv_taps[layer_idx])
        total_sum, total_squares = (
            taken_together(jnp.sum(conved, axis=1), "tp"),
            taken_together(jnp.sum(conved * conved, axis=1), "tp"),
        )
        row_mean = total_sum / C
        spread = total_squares / C - row_mean * row_mean
        normed = (conved - row_mean[:, None]) * lax.rsqrt(spread + epsilon)[:, None] * norm_gain[
            layer_idx
        ] + norm_shift[layer_idx]
        mixed_out = jax.nn.silu(normed).astype(jnp.bfloat16)
        partial_value = jnp.dot(
            mixed_out,
            lax.all_gather(w_out[layer_idx], "sp", axis=1, tiled=True),
            preferred_element_type=jnp.float32,
        )
        summed = lax.psum_scatter(
            partial_value.astype(jnp.bfloat16), "tp", scatter_dimension=1, tiled=True
        ).astype(jnp.float32)
        current = (residual.astype(jnp.float32) + summed).astype(jnp.bfloat16)
    return current


def solution(mesh):
    placed = (
        P(("grp", "sp"), "tp"),
        P(None, "tp"),
        P(None, "sp", "tp"),
        P(None, "sp", "tp"),
        P(None, None, "tp"),
        P(None, "tp"),
        P(None, "tp"),
        P(None, "tp", "sp"),
    )
    return jax.shard_map(
        shards, mesh=mesh, in_specs=placed, out_specs=P(("grp", "sp"), "tp"), check_vma=False
    )
```

profile of v0, /device:TPU:33, one launch (start us, length us, event | category | flops | bytes accessed | tf_op | source)
XLA Modules:
  0.0 419.5 jit_solution(574463797681582557)
XLA Ops:
  6.6 1.8 slice_bitcast_fusion
  8.4 0.7 pad_maximum_fusion
  9.1 0.1 all-gather.7.cloned.1.call-update
  9.2 1.2 fusion.46
  10.3 0.6 broadcast_in_dim.20
  10.9 23.6 %all-to-all-start = ((f32[8,1,384]{2,1,0:T(1,128)}), f32[8,1,384]{2,1,0:T(1,128)S(1)}, u32[]{:S(2)}, u32[]{:S(2)}) async-start(f32[8,1,384]{2,1,0:T(1,128)} %broadcast_in_dim.20), calls=%async_computation | async-start | bytes 24576 | tf_op jit(solution)/shard_map/all_to_all | solution.py:15
  34.6 0.8 fusion.101
  35.3 3.9 all-to-all-done
  39.3 1.2 fusion.48
  40.5 0.2 copy.32
  40.7 1.9 broadcast_in_dim.21
  42.6 4.4 %all-to-all-start.1 = ((bf16[8,384,512]{1,2,0:T(8,128)(2,1)}), bf16[8,384,512]{1,2,0:T(8,128)(2,1)S(1)}, u32[]{:S(2)}, u32[]{:S(2)}) async-start(bf16[8,384,512]{1,2,0:T(8,128)(2,1)} %broadcast_in_dim.21), calls=%async_computation.1 | async-start | bytes 6291456 | tf_op jit(solution)/shard_map/all_to_all | solution.py:15
  47.0 0.7 fusion.100
  47.8 0.1 all-gather.11.cloned.1.call-update
  47.8 36.7 %all-to-all-done.1 = bf16[8,384,512]{1,2,0:T(8,128)(2,1)S(1)} async-done(((bf16[8,384,512]{1,2,0:T(8,128)(2,1)}), bf16[8,384,512]{1,2,0:T(8,128)(2,1)S(1)}, u32[]{:S(2)}, u32[]{:S(2)}) %all-to-all-start.1) | async-done | bytes 3145760 | tf_op jit(solution)/shard_map/all_to_all | solution.py:15
  84.5 6.8 %all-gather.7.cloned.1.call-done = bf16[4096,512]{1,0:T(8,128)(2,1)} async-done(((bf16[256,512]{1,0:T(8,128)(2,1)}), bf16[4096,512]{1,0:T(8,128)(2,1)}) %all-gather.7.cloned.1.call-update) | async-done | bytes 4194320 | tf_op jit(solution)/shard_map/all_gather | solution.py:39
  91.4 2.8 fusion.37
  94.2 1.0 fusion.43
  95.2 2.1 collective-permute-start
  97.4 0.8 collective-permute-done
  98.5 1.8 convolution_select_fusion.1
  100.3 0.1 copy.35
  100.5 0.1 slice_reduce_fusion.1
  100.6 0.6 broadcast_in_dim.23
  101.2 15.5 %all-to-all-start.2 = ((f32[8,1,384]{2,1,0:T(1,128)}), f32[8,1,384]{2,1,0:T(1,128)S(1)}, u32[]{:S(2)}, u32[]{:S(2)}) async-start(f32[8,1,384]{2,1,0:T(1,128)} %broadcast_in_dim.23), calls=%async_computation.2 | async-start | bytes 24576 | tf_op jit(solution)/shard_map/all_to_all | solution.py:15
  116.7 0.1 fusion.63
  116.8 4.5 %all-to-all-done.2 = f32[8,1,384]{2,1,0:T(1,128)S(1)} async-done(((f32[8,1,384]{2,1,0:T(1,128)}), f32[8,1,384]{2,1,0:T(1,128)S(1)}, u32[]{:S(2)}, u32[]{:S(2)}) %all-to-all-start.2) | async-done | bytes 12320 | tf_op jit(solution)/shard_map/all_to_all | solution.py:15
  121.3 0.6 broadcast_in_dim.24
  121.9 4.0 all-to-all-start.3
  125.9 4.8 %all-to-all-done.3 = f32[8,1,384]{2,1,0:T(1,128)S(1)} async-done(((f32[8,1,384]{2,1,0:T(1,128)}), f32[8,1,384]{2,1,0:T(1,128)S(1)}, u32[]{:S(2)}, u32[]{:S(2)}) %all-to-all-start.3) | async-done | bytes 12320 | tf_op jit(solution)/shard_map/all_to_all | solution.py:15
  130.7 33.4 %all-gather.11.cloned.1.call-done = bf16[1,256,4096]{2,1,0:T(8,128)(2,1)} async-done(((bf16[1,256,256]{2,1,0:T(8,128)(2,1)}), bf16[1,256,4096]{2,1,0:T(8,128)(2,1)}) %all-gather.11.cloned.1.call-update) | async-done | bytes 2097168 | tf_op jit(solution)/shard_map/all_gather | solution.py:94
  164.2 4.3 %convolution_convert_fusion.1 = bf16[384,4096]{1,0:T(8,128)(2,1)} fusion(bf16[1,256,4096]{2,1,0:T(8,128)(2,1)} %all-gather.11.cloned.1.call-done, f32[1,416,256]{2,1,0:T(8,128)S(1)} %reshape.86, f32[256]{0:T(256)S(1)} %bitcast.83, f32[256]{0:T(256)S(1)} %bitcast.82, f32[384]{0:T(512)S(1)} %get-tuple-element.20, f32[384]{0:T(512)S(1)} %get-tuple-element.19), kind=kOutput, calls=%fused_computation.1 | convolution fusion | flops 807763968 | bytes 5642240 | tf_op jit(solution)/shard_map/dot_general | solution.py:92
  168.5 0.1 reduce-scatter.3.cloned.1.call-update
  168.6 0.1 all-gather.9.cloned.1.call-start
  168.6 0.8 copy-done.2
  169.4 0.1 copy-done.3
  169.5 0.7 pad_maximum_fusion.1
  170.2 45.8 %reduce-scatter.3.cloned.1.call-done = bf16[384,512]{1,0:T(8,128)(2,1)} async-done(((bf16[384,4096]{1,0:T(8,128)(2,1)}), bf16[384,512]{1,0:T(8,128)(2,1)}) %reduce-scatter.3.cloned.1.call-update) | async-done | bytes 393232 | tf_op jit(solution)/shard_map/reduce_scatter | solution.py:97
  216.1 1.2 fusion.50
  217.3 9.8 %all_to_all.46 = f32[8,1,384]{2,1,0:T(1,128)S(1)} all-to-all(f32[8,1,384]{2,1,0:T(1,128)S(1)} %broadcast_in_dim.25), channel_id=1, replica_groups=mesh['grp'=2,'sp'=16,'tp'=8] {'tp'}, dimensions={0} | all-to-all | bytes 24576 | tf_op jit(solution)/shard_map/all_to_all | solution.py:15
  227.2 1.2 fusion.52
  228.4 0.2 copy.39
  228.6 1.9 broadcast_in_dim.26
  230.5 4.3 %all-to-all-start.5 = ((bf16[8,384,512]{1,2,0:T(8,128)(2,1)}), bf16[8,384,512]{1,2,0:T(8,128)(2,1)S(1)}, u32[]{:S(2)}, u32[]{:S(2)}) async-start(bf16[8,384,512]{1,2,0:T(8,128)(2,1)} %broadcast_in_dim.26), calls=%async_computation.6 | async-start | bytes 6291456 | tf_op jit(solution)/shard_map/all_to_all | solution.py:15
  234.8 0.6 all-gather.13.cloned.1.call-update
  235.4 50.7 %all-gather.9.cloned.1.call-done = bf16[4096,512]{1,0:T(8,128)(2,1)} async-done(((bf16[256,512]{1,0:T(8,128)(2,1)}), bf16[4096,512]{1,0:T(8,128)(2,1)}) %all-gather.9.cloned.1.call-update) | async-done | bytes 4194320 | tf_op jit(solution)/shard_map/all_gather | solution.py:39
  286.1 2.8 fusion.31
  289.0 1.1 fusion.40
  290.1 2.6 collective-permute-start.1
  292.7 0.7 collective-permute-done.1
  293.6 1.8 convolution_select_fusion
  295.4 0.1 copy.42
  295.6 0.1 slice_reduce_fusion
  295.8 0.6 broadcast_in_dim.28
  296.4 15.3 %all-to-all-start.6 = ((f32[8,1,384]{2,1,0:T(1,128)}), f32[8,1,384]{2,1,0:T(1,128)S(1)}, u32[]{:S(2)}, u32[]{:S(2)}) async-start(f32[8,1,384]{2,1,0:T(1,128)} %broadcast_in_dim.28), calls=%async_computation.7 | async-start | bytes 24576 | tf_op jit(solution)/shard_map/all_to_all | solution.py:15
  311.7 0.1 fusion.59
  311.8 4.5 %all-to-all-done.6 = f32[8,1,384]{2,1,0:T(1,128)S(1)} async-done(((f32[8,1,384]{2,1,0:T(1,128)}), f32[8,1,384]{2,1,0:T(1,128)S(1)}, u32[]{:S(2)}, u32[]{:S(2)}) %all-to-all-start.6) | async-done | bytes 12320 | tf_op jit(solution)/shard_map/all_to_all | solution.py:15
  316.3 0.6 broadcast_in_dim.29
  316.9 4.0 all-to-all-start.7
  320.9 4.8 %all-to-all-done.7 = f32[8,1,384]{2,1,0:T(1,128)S(1)} async-done(((f32[8,1,384]{2,1,0:T(1,128)}), f32[8,1,384]{2,1,0:T(1,128)S(1)}, u32[]{:S(2)}, u32[]{:S(2)}) %all-to-all-start.7) | async-done | bytes 12320 | tf_op jit(solution)/shard_map/all_to_all | solution.py:15
  325.7 33.5 %all-gather.13.cloned.1.call-done = bf16[1,256,4096]{2,1,0:T(8,128)(2,1)} async-done(((bf16[1,256,256]{2,1,0:T(8,128)(2,1)}), bf16[1,256,4096]{2,1,0:T(8,128)(2,1)}) %all-gather.13.cloned.1.call-update) | async-done | bytes 2097168 | tf_op jit(solution)/shard_map/all_gather | solution.py:94
  359.2 4.3 %convolution_convert_fusion = bf16[384,4096]{1,0:T(8,128)(2,1)} fusion(bf16[1,256,4096]{2,1,0:T(8,128)(2,1)} %all-gather.13.cloned.1.call-done, f32[1,416,256]{2,1,0:T(8,128)S(1)} %reshape.93, f32[256]{0:T(256)S(1)} %bitcast.81, f32[256]{0:T(256)S(1)} %bitcast.80, f32[384]{0:T(512)S(1)} %get-tuple-element.14, f32[384]{0:T(512)S(1)} %get-tuple-element.13), kind=kOutput, calls=%fused_computation | convolution fusion | flops 807763968 | bytes 5642240 | tf_op jit(solution)/shard_map/dot_general | solution.py:92
  363.6 47.2 %reduce-scatter.5.cloned.1.call-done = bf16[384,512]{1,0:T(8,128)(2,1)} async-done(((bf16[384,4096]{1,0:T(8,128)(2,1)}), bf16[384,512]{1,0:T(8,128)(2,1)}) %reduce-scatter.5.cloned.1.call-update) | async-done | bytes 393232 | tf_op jit(solution)/shard_map/reduce_scatter | solution.py:97
  410.8 1.9 fusion.53
  (55 shorter events, 0.9 us)
Async XLA Ops:
  6.5 84.8 %all-gather.7.cloned.1.call-start = ((), (), s32[]{:S(2)}) async-start(), calls=%async_computation.10 | async-start | bytes 4456448 | tf_op jit(solution)/shard_map/all_gather | solution.py:39
  10.9 28.3 %all-to-all-start = ((f32[8,1,384]{2,1,0:T(1,128)}), f32[8,1,384]{2,1,0:T(1,128)S(1)}, u32[]{:S(2)}, u32[]{:S(2)}) async-start(f32[8,1,384]{2,1,0:T(1,128)} %broadcast_in_dim.20), calls=%async_computation | async-start | bytes 24576 | tf_op jit(solution)/shard_map/all_to_all | solution.py:15
  42.6 4.4 %copy-start.4 = (bf16[2,256,256]{2,1,0:T(8,128)(2,1)S(1)}, bf16[2,256,256]{2,1,0:T(8,128)(2,1)}, u32[]{:S(2)}) copy-start(bf16[2,256,256]{2,1,0:T(8,128)(2,1)} %param.15) | copy-start | bytes 786436
  42.6 41.9 %all-to-all-start.1 = ((bf16[8,384,512]{1,2,0:T(8,128)(2,1)}), bf16[8,384,512]{1,2,0:T(8,128)(2,1)S(1)}, u32[]{:S(2)}, u32[]{:S(2)}) async-start(bf16[8,384,512]{1,2,0:T(8,128)(2,1)} %broadcast_in_dim.21), calls=%async_computation.1 | async-start | bytes 6291456 | tf_op jit(solution)/shard_map/all_to_all | solution.py:15
  47.0 117.1 %all-gather.11.cloned.1.call-start = ((), (), s32[]{:S(2)}) async-start(), calls=%async_computation.14 | async-start | bytes 2228224 | tf_op jit(solution)/shard_map/all_gather | solution.py:94
  91.4 2.8 copy-start.7
  94.2 3.2 copy-start.5
  94.2 4.3 %copy-start.9 = (pred[8,52]{0,1:T(8,128)(4,1)S(1)}, pred[8,52]{0,1:T(8,128)(4,1)}, u32[]{:S(2)}) copy-start(pred[8,52]{0,1:T(8,128)(4,1)} %constant.31) | copy-start | bytes 1252
  95.2 3.0 collective-permute-start
  98.5 27.4 %copy-start.6 = (f32[2,256]{1,0:T(2,128)S(1)}, f32[2,256]{1,0:T(2,128)}, u32[]{:S(2)}) copy-start(f32[2,256]{1,0:T(2,128)} %param.14) | copy-start | bytes 6148
  101.2 20.1 %all-to-all-start.2 = ((f32[8,1,384]{2,1,0:T(1,128)}), f32[8,1,384]{2,1,0:T(1,128)S(1)}, u32[]{:S(2)}, u32[]{:S(2)}) async-start(f32[8,1,384]{2,1,0:T(1,128)} %broadcast_in_dim.23), calls=%async_computation.2 | async-start | bytes 24576 | tf_op jit(solution)/shard_map/all_to_all | solution.py:15
  121.9 8.8 %all-to-all-start.3 = ((f32[8,1,384]{2,1,0:T(1,128)}), f32[8,1,384]{2,1,0:T(1,128)S(1)}, u32[]{:S(2)}, u32[]{:S(2)}) async-start(f32[8,1,384]{2,1,0:T(1,128)} %broadcast_in_dim.24), calls=%async_computation.3 | async-start | bytes 24576 | tf_op jit(solution)/shard_map/all_to_all | solution.py:15
  125.9 90.2 %reduce-scatter.3.cloned.1.call-start = ((), (), s32[]{:S(2)}) async-start(), calls=%async_computation.11 | async-start | bytes 3538944 | tf_op jit(solution)/shard_map/reduce_scatter | solution.py:97
  168.5 0.9 copy-start.2
  168.5 1.0 copy-start.3
  168.5 47.6 %copy-start = (bf16[384,512]{1,0:T(8,128)(2,1)S(1)}, bf16[384,512]{1,0:T(8,128)(2,1)}, u32[]{:S(2)}) copy-start(bf16[384,512]{1,0:T(8,128)(2,1)} %param.8) | copy-start | bytes 1179652
  168.6 117.6 %all-gather.9.cloned.1.call-start = ((), (), s32[]{:S(2)}) async-start(), calls=%async_computation.12 | async-start | bytes 4456448 | tf_op jit(solution)/shard_map/all_gather | solution.py:39
  230.5 55.6 %all-to-all-start.5 = ((bf16[8,384,512]{1,2,0:T(8,128)(2,1)}), bf16[8,384,512]{1,2,0:T(8,128)(2,1)S(1)}, u32[]{:S(2)}, u32[]{:S(2)}) async-start(bf16[8,384,512]{1,2,0:T(8,128)(2,1)} %broadcast_in_dim.26), calls=%async_computation.6 | async-start | bytes 6291456 | tf_op jit(solution)/shard_map/all_to_all | solution.py:15
  234.8 124.4 %all-gather.13.cloned.1.call-start = ((), (), s32[]{:S(2)}) async-start(), calls=%async_computation.15 | async-start | bytes 2228224 | tf_op jit(solution)/shard_map/all_gather | solution.py:94
  286.1 2.8 copy-start.8
  289.0 4.6 %copy-start.10 = (pred[8,52]{0,1:T(8,128)(4,1)S(1)}, pred[8,52]{0,1:T(8,128)(4,1)}, u32[]{:S(2)}) copy-start(pred[8,52]{0,1:T(8,128)(4,1)} %constant.31) | copy-start | bytes 1252
  290.1 3.3 collective-permute-start.1
  296.4 19.9 %all-to-all-start.6 = ((f32[8,1,384]{2,1,0:T(1,128)}), f32[8,1,384]{2,1,0:T(1,128)S(1)}, u32[]{:S(2)}, u32[]{:S(2)}) async-start(f32[8,1,384]{2,1,0:T(1,128)} %broadcast_in_dim.28), calls=%async_computation.7 | async-start | bytes 24576 | tf_op jit(solution)/shard_map/all_to_all | solution.py:15
  316.9 8.8 %all-to-all-start.7 = ((f32[8,1,384]{2,1,0:T(1,128)}), f32[8,1,384]{2,1,0:T(1,128)S(1)}, u32[]{:S(2)}, u32[]{:S(2)}) async-start(f32[8,1,384]{2,1,0:T(1,128)} %broadcast_in_dim.29), calls=%async_computation.8 | async-start | bytes 24576 | tf_op jit(solution)/shard_map/all_to_all | solution.py:15
  320.9 89.9 %reduce-scatter.5.cloned.1.call-start = ((), (), s32[]{:S(2)}) async-start(), calls=%async_computation.13 | async-start | bytes 3538944 | tf_op jit(solution)/shard_map/reduce_scatter | solution.py:97
  363.5 47.3 %copy-start.1 = (bf16[384,512]{1,0:T(8,128)(2,1)S(1)}, bf16[384,512]{1,0:T(8,128)(2,1)}, u32[]{:S(2)}) copy-start(bf16[384,512]{1,0:T(8,128)(2,1)} %reduce-scatter.3.cloned.1.call-done) | copy-start | bytes 1179652
Sparse Core Ops, SparseCore 0:
  9.3 82.0 all-gather.6
  93.1 71.0 all-gather.10
  168.7 47.3 reduce-scatter.2
  217.7 68.3 all-gather.8
  287.7 71.4 all-gather.12
  363.7 47.0 reduce-scatter.4
where the time goes:
time: 421 us; the launch traced here: 420 us
  waiting for transfers between devices  279 us (66%)
  starting transfers between devices  75.8 us (18%)
  matrix products  19.9 us (5%)
  between operations  13.8 us (3%)
  local copies, waits for them, and re-layouts  12.2 us (3%)
  blocking collectives  9.85 us (2%)
  other arithmetic  8.91 us (2%)
    reduce_scatter x2, waiting for transfers between devices, shards(): lax.psum_scatter(partial_value.astype(jnp.bfloat16), 'tp', scatter_dimens...  93 us
    all_to_all x7, starting transfers between devices, from_everyone(): lax.all_to_all(jnp.broadcast_to(x[None], (size, *x.shape)), axis, 0, 0, t...  71 us
    all_gather x2, waiting for transfers between devices, shards(): lax.all_gather(w_out[layer_idx], 'sp', axis=1, tiled=True)  66.9 us
    all_to_all x7, waiting for transfers between devices, from_everyone(): lax.all_to_all(jnp.broadcast_to(x[None], (size, *x.shape)), axis, 0, 0, t...  59.2 us
    all_gather x2, waiting for transfers between devices, side_by_side(): lax.all_gather(both, axis, axis=dim, tiled=True)  57.5 us
    all_to_all x1, blocking collectives, from_everyone(): lax.all_to_all(jnp.broadcast_to(x[None], (size, *x.shape)), axis, 0, 0, t...  9.85 us
    dot_general x2, matrix products, shards(): jnp.dot(mixed_out, lax.all_gather(w_out[layer_idx], 'sp', axis=1, tiled=T...  8.62 us
  transfers between devices with their start and end apart: 15, of which 14 were waited for; matrix products, arithmetic and copies ran while one was open for 6% of the time, Pallas kernels for 0%

commit v1 on v0

v1 whole, which is shorter than its diff:
```python
import functools

import jax
import jax.numpy as jnp
from jax import lax
from jax.experimental import pallas as pl
from jax.experimental.pallas import tpu as pltpu
from jax.sharding import PartitionSpec as P

MESH = pl.DeviceIdType.MESH
EPS = 1e-06
F32 = jnp.float32
BF16 = jnp.bfloat16
RIGHT, LEFT = 1, -1


def mm(a, b):
    return jnp.dot(a, b, preferred_element_type=F32)


def both(col):
    return jnp.concatenate([col, col], axis=1)


def kernel(
    sizes,
    hidden,
    in_gain,
    w_value,
    w_gate,
    taps,
    norm_gain,
    norm_shift,
    w_out,
    out,
    wbuf,
    xg,
    cur,
    acc_v,
    acc_g,
    col_a,
    col_b,
    rstat,
    cstat,
    halo_out,
    halo_in,
    ext,
    shifted,
    conved,
    mixed,
    p_out,
    p_in,
    c_out,
    c_in,
    local_sem,
    z_send,
    z_recv,
    y_send,
    y_recv,
    x_send,
    x_recv,
    s_send,
    s_recv,
    h_send,
    h_recv,
    p_send,
    p_recv,
    c_send,
    c_recv,
):
    groups, ns, nt = sizes
    layers = w_value.shape[0]
    rows_w, ch = w_value.shape[1], w_value.shape[2]
    tokens = hidden.shape[0]
    n_taps = taps.shape[1]
    nx = nt // 2
    half = ns // 2
    channels = ch * nt
    features = hidden.shape[1] * nt
    z = lax.axis_index("sp")
    t = lax.axis_index("tp")
    paired = groups % 2 == 0
    x, c = t // 2, lax.rem(t, 2)

    def chip(dx, core):
        return 2 * lax.rem(x + dx + nx, nx) + core

    t_right, t_left, t_opp, t_mate = chip(1, c), chip(-1, c), chip(2, c), 2 * x + (1 - c)

    if paired:
        y = lax.axis_index("grp")
        par = lax.rem(y, 2)
        y_mate = y + 1 - 2 * par
        lone = 80
        ring_rows = rows_w - lone
        ring_at = pl.ds(pl.multiple_of(par * lone, 16), ring_rows)
        y_out_at = pl.ds(pl.multiple_of(par * ring_rows, 16), lone)
        y_in_at = pl.ds(pl.multiple_of((1 - par) * ring_rows, 16), lone)
    else:
        ring_at = pl.ds(0, rows_w)

    def zc(offset):
        return lax.rem(z + offset + 2 * ns, ns)

    def remote(src, dst, ssem, rsem, **where):
        return pltpu.make_async_remote_copy(
            src_ref=src, dst_ref=dst, send_sem=ssem, recv_sem=rsem, device_id=where, device_id_type=MESH
        )

    def z_copy(l, sub, d, s):
        at = wbuf.at[l, zc(-d * (s - 1)), sub, ring_at, :]
        way = 0 if d == RIGHT else 1
        return remote(at, at, z_send.at[l, sub, way, s % 2], z_recv.at[l, sub, way, s - 1], sp=zc(d))

    def z_arrival(l, sub, d, s):
        at = wbuf.at[l, zc(-d * s), sub, ring_at, :]
        way = 0 if d == RIGHT else 1
        return remote(at, at, z_send.at[l, sub, way, s % 2], z_recv.at[l, sub, way, s - 1], sp=zc(d))

    def active(l, sub, d, s):
        if s < half:
            return True
        return s == half and d == (RIGHT, LEFT, RIGHT if l % 2 == 0 else LEFT)[sub]

    def y_copy(l, chunk, slot, rows):
        at = wbuf.at[l, chunk, :, rows, :]
        return remote(at, at, y_send.at[l, slot], y_recv.at[l, slot], grp=y_mate)

    def hop_chunks(s):
        if s == 0:
            return [(zc(0), None)]
        if s == half:
            return [(zc(half), ns - 2)]
        return [(zc(-s), 2 * s - 2), (zc(s), 2 * s - 1)]

    def z_first(l):
        for sub in range(3):
            for d in (RIGHT, LEFT):
                if active(l, sub, d, 1):
                    z_copy(l, sub, d, 1).start()

    def serve(l, s):
        for sub in range(3):
            for d in (RIGHT, LEFT):
                if not active(l, sub, d, s):
                    continue
                z_arrival(l, sub, d, s).wait_recv()
                if active(l, sub, d, s + 1):
                    if s >= 2:
                        z_copy(l, sub, d, s - 1).wait_send()
                    z_copy(l, sub, d, s + 1).start()
        if paired:
            for chunk, slot in hop_chunks(s):
                y_copy(l, chunk, slot, y_out_at).start()

    def z_drain(l):
        for sub in range(3):
            for d in (RIGHT, LEFT):
                last = half if active(l, sub, d, half) else half - 1
                for s in range(max(1, last - 1), last + 1):
                    z_copy(l, sub, d, s).wait_send()

    def y_wait(l, s):
        if paired and s > 0:
            for chunk, slot in hop_chunks(s):
                y_copy(l, chunk, slot, y_in_at).wait_recv()

    def y_drain(l):
        if paired:
            for s in range(1, half + 1):
                for chunk, slot in hop_chunks(s):
                    y_copy(l, chunk, slot, y_out_at).wait_send()

    def x_copy(l, chunk, slot, to):
        at = xg.at[l, chunk]
        return remote(at, at, x_send.at[l, slot], x_recv.at[l, chunk], tp=to)

    def x_begin(l):
        a, b = 2 * t, 2 * t + 1
        sends = ((a, 0, t_right), (b, 1, t_left), (b, 2, t_right), (a, 3, t_left), (a, 4, t_mate), (b, 5, t_mate))
        for chunk, slot, to in sends:
            x_copy(l, chunk, slot, to).start()
        return sends

    def x_middle(l):
        a, b, e, f = 2 * t_left, 2 * t_right + 1, 2 * t_left + 1, 2 * t_right
        sends = ((a, 6, t_right), (a, 7, t_mate), (b, 8, t_left), (b, 9, t_mate), (e, 10, t_mate), (f, 11, t_mate))
        arrived = []
        for chunk, slot, to in sends:
            if not any(chunk is other for other in arrived):
                x_copy(l, chunk, slot, to).wait_recv()
                arrived.append(chunk)
            x_copy(l, chunk, slot, to).start()
        return sends

    def x_far(l):
        a, b = 2 * t_opp, 2 * t_opp + 1
        sends = ((a, 12, t_mate), (b, 13, t_mate))
        for chunk, slot, to in sends:
            x_copy(l, chunk, slot, to).wait_recv()
            x_copy(l, chunk, slot, to).start()
        return sends

    def x_mate_wait(l, dx):
        for h in range(2):
            x_copy(l, 2 * chip(dx, 1 - c) + h, 0, t_mate).wait_recv()

    def stat_copies(buf, l, kind):
        copies = []
        for j in range(1, nt):
            to = lax.rem(t + j, nt)
            at = buf.at[l, t]
            copies.append(remote(at, at, s_send.at[l, kind, j - 1], s_recv.at[l, kind, j - 1], tp=to))
        return copies

    def stat_wait(buf, l, kind):
        for j in range(1, nt):
            at = buf.at[l, lax.rem(t + nt - j, nt)]
            remote(at, at, s_send.at[l, kind, j - 1], s_recv.at[l, kind, j - 1], tp=t_mate).wait_recv()

    def to_lanes(column):
        return jnp.broadcast_to(column, (tokens, 128)).T[:8]

    def to_column(row):
        return jnp.broadcast_to(row[:1], (128, tokens)).T

    def prepare(l):
        value = cur[...]
        squares = jnp.sum(value * value, axis=1, keepdims=True)
        rstat[l, t] = to_lanes(squares)
        scaled = (value * in_gain[l : l + 1, :]).astype(BF16)
        xg[l, 2 * t] = scaled[:, : scaled.shape[1] // 2]
        xg[l, 2 * t + 1] = scaled[:, scaled.shape[1] // 2 :]

    def accumulate(l, chunks, first):
        for sub, acc in ((0, acc_v), (1, acc_g)):
            total = None if first else acc[...]
            for chunk in chunks:
                part = mm(xg[l, chunk], wbuf[l, chunk, sub])
                total = part if total is None else total + part
            acc[...] = total

    block = 96

    def over_rows(body):
        def step(i, carry):
            body(pl.multiple_of(i * block, block))
            return carry

        lax.fori_loop(0, tokens // block, step, 0)

    def halo_copy(l):
        return remote(halo_out.at[l], halo_in.at[l], h_send.at[l], h_recv.at[l], sp=zc(1))

    reach = halo_out.shape[1]

    def gate(l):
        stat_wait(rstat, l, 0)
        total = rstat[l, 0]
        for j in range(1, nt):
            total = total + rstat[l, j]
        col_a[...] = to_column(lax.rsqrt(total / features + EPS))

        def body(at):
            rows = pl.ds(at, block)
            scale = both(col_a[rows, :])
            value = acc_v[rows, :] * scale
            gated = value * jax.nn.sigmoid(acc_g[rows, :] * scale)
            ext[pl.ds(pl.multiple_of(at + reach, 32), block), :] = gated.astype(BF16).astype(F32)

        over_rows(body)
        halo_out[l] = ext[tokens : tokens + reach, :].astype(BF16)
        halo_copy(l).start()

    def convolve(l):
        halo_copy(l).wait_recv()
        before = halo_in[l].astype(F32)
        ext[:reach, :] = jnp.where(z > 0, before, jnp.zeros_like(before))
        span = shifted.shape[1]
        for b in range(1, 8):
            shifted[b - 1] = ext[b : b + span, :]
        offset = reach - (n_taps - 1)

        def body(at):
            total = jnp.zeros((block // 4, ch), F32)
            return total

        small = 32

        def step(i, carry):
            at = pl.multiple_of(i * small, small)
            total = jnp.zeros((small, ch), F32)
            for k in range(n_taps):
                o = k + offset
                a, b = (o // 8) * 8, o % 8
                rows = pl.ds(pl.multiple_of(at + a, 8), small)
                window = ext[rows, :] if b == 0 else shifted[b - 1, rows, :]
                total = total + taps[l, k : k + 1, :] * window
            conved[pl.ds(at, small), :] = total
            return carry

        lax.fori_loop(0, tokens // small, step, 0)
        value = conved[...]
        sums = jnp.sum(value, axis=1, keepdims=True)
        spread = value - sums / ch
        cstat[l, t, :8] = to_lanes(sums)
        cstat[l, t, 8:] = to_lanes(jnp.sum(spread * spread, axis=1, keepdims=True))
        for copy in stat_copies(cstat, l, 1):
            copy.start()

    def normalize(l):
        stat_wait(cstat, l, 1)
        total = cstat[l, 0, :8]
        for j in range(1, nt):
            total = total + cstat[l, j, :8]
        mean = total / channels
        spread = jnp.zeros_like(mean)
        for j in range(nt):
            away = cstat[l, j, :8] / ch - mean
            spread = spread + (cstat[l, j, 8:] + ch * (away * away))
        col_a[...] = to_column(mean)
        col_b[...] = to_column(lax.rsqrt(spread / channels + EPS))

        def body(at):
            rows = pl.ds(at, block)
            normed = (conved[rows, :] - both(col_a[rows, :])) * both(col_b[rows, :])
            normed = normed * norm_gain[l : l + 1, :] + norm_shift[l : l + 1, :]
            mixed[rows, :] = (normed / (1.0 + jnp.exp(-normed))).astype(BF16)

        over_rows(body)

    def project(l, dx, core, h):
        return mm(mixed[...], wbuf[l, 2 * chip(dx, core) + h, 2])

    def p_copy(l, q):
        return remote(p_out.at[l, q], p_in.at[l, q], p_send.at[l, q], p_recv.at[l, q], tp=t_mate)

    def c_copy(l, slot):
        to = t_right if slot in (0, 2, 3) else t_left
        return remote(c_out.at[l, slot], c_in.at[l, slot], c_send.at[l, slot], c_recv.at[l, slot], tp=to)

    def give(l, dx, h):
        q = 2 * dx + h
        p_out[l, q] = project(l, dx, 1 - c, h).astype(BF16)
        p_copy(l, q).start()

    def pass_on(l, dx, h, slot, extra=None):
        q = 2 * dx + h
        total = project(l, dx, c, h)
        p_copy(l, q).wait_recv()
        total = total + p_in[l, q].astype(F32)
        if extra is not None:
            c_copy(l, extra).wait_recv()
            total = total + c_in[l, extra].astype(F32)
        c_out[l, slot] = total.astype(BF16)
        c_copy(l, slot).start()

    def settle(l, h, last):
        total = project(l, 0, c, h)
        p_copy(l, h).wait_recv()
        total = total + p_in[l, h].astype(F32)
        for slot in (2 + h, 4 + h):
            c_copy(l, slot).wait_recv()
            total = total + c_in[l, slot].astype(F32)
        cols = slice(h * ch, (h + 1) * ch)
        new = (cur[:, cols] + total).astype(BF16)
        if last:
            out[:, cols] = new
        else:
            cur[:, cols] = new.astype(F32)

    barrier = pltpu.get_barrier_semaphore()
    greeted = [{"tp": lax.rem(t + j, nt)} for j in range(1, nt)]
    greeted += [{"sp": zc(1)}, {"sp": zc(-1)}]
    if paired:
        greeted += [{"grp": y_mate}]
    for where in greeted:
        pl.semaphore_signal(barrier, inc=1, device_id=where, device_id_type=MESH)

    def local(l, sub):
        src = (w_value, w_gate, w_out)[sub]
        return pltpu.make_async_copy(src.at[l], wbuf.at[l, z, sub], local_sem.at[l, sub])

    for l in range(layers):
        for sub in range(3):
            local(l, sub).start()
    for sub in range(3):
        local(0, sub).wait()
    pl.semaphore_wait(barrier, len(greeted))

    z_first(0)
    cur[...] = hidden[...].astype(F32)
    prepare(0)
    x_sends = [[] for _ in range(layers)]
    x_sends[0] += x_begin(0)
    for copy in stat_copies(rstat, 0, 0):
        copy.start()
    serve(0, 1)
    x_sends[0] += x_middle(0)
    serve(0, 2)
    x_sends[0] += x_far(0)
    for dx in range(nx):
        x_mate_wait(0, dx)

    def ring_mm(l, s):
        y_wait(l, s)
        accumulate(l, [chunk for chunk, _ in hop_chunks(s)], s == 0)

    ring_mm(0, 0)
    ring_mm(0, 1)
    for s in range(3, half + 1):
        serve(0, s)
        if s == half - 1 and layers > 1:
            for sub in range(3):
                local(1, sub).wait()
            z_first(1)
        ring_mm(0, s - 1)
    ring_mm(0, half)

    for l in range(layers):
        last = l == layers - 1

        def more(s):
            if not last:
                serve(l + 1, s)

        gate(l)
        more(1)
        convolve(l)
        more(2)
        normalize(l)
        if last:
            for s in range(1, half + 1):
                pass
        give(l, 2, 0)
        give(l, 2, 1)
        give(l, 1, 1)
        pass_on(l, 2, 0, 0)
        pass_on(l, 2, 1, 1)
        give(l, 3, 0)
        pass_on(l, 1, 1, 3)
        give(l, 1, 0)
        pass_on(l, 3, 0, 4)
        more(3)
        give(l, 3, 1)
        give(l, 0, 0)
        give(l, 0, 1)
        pass_on(l, 1, 0, 2, 0)
        pass_on(l, 3, 1, 5, 1)
        more(4)
        settle(l, 0, last)
        settle(l, 1, last)
        if not last:
            n = l + 1
            prepare(n)
            x_sends[n] += x_begin(n)
            for copy in stat_copies(rstat, n, 0):
                copy.start()
            more(5)
            accumulate_done = False
            x_sends[n] += x_middle(n)
            more(6)
            x_sends[n] += x_far(n)
            more(7)
            more(8)
            for s in range(1, half + 1):
                y_wait(n, s)
            first = True
            for dx in (0, 1, -1, 2):
                accumulate(n, [2 * chip(dx, c), 2 * chip(dx, c) + 1], first)
                first = False
            for dx in (0, 1, -1, 2):
                x_mate_wait(n, dx)
                accumulate(n, [2 * chip(dx, 1 - c), 2 * chip(dx, 1 - c) + 1], False)

    for l in range(layers):
        z_drain(l)
        y_drain(l)
        for chunk, slot, to in x_sends[l]:
            x_copy(l, chunk, slot, to).wait_send()
        for copy in stat_copies(rstat, l, 0) + stat_copies(cstat, l, 1):
            copy.wait_send()
        halo_copy(l).wait_send()
        for q in range(2 * nx):
            p_copy(l, q).wait_send()
        for slot in range(6):
            c_copy(l, slot).wait_send()


def solution(mesh):
    sizes = (mesh.shape["grp"], mesh.shape["sp"], mesh.shape["tp"])
    groups, ns, nt = sizes

    def shards(hidden_in, in_gain, w_value, w_gate, conv_taps, norm_gain, norm_shift, w_out):
        layers, rows_w, ch = w_value.shape
        tokens = hidden_in.shape[0]
        vmem = pltpu.VMEM
        dma = pltpu.SemaphoreType.DMA
        half = ns // 2
        scratch = [
            vmem((layers, ns, 3, rows_w, ch), BF16),
            vmem((layers, 2 * nt, tokens, ch), BF16),
            vmem((tokens, 2 * ch), F32),
            vmem((tokens, ch), F32),
            vmem((tokens, ch), F32),
            vmem((tokens, 128), F32),
            vmem((tokens, 128), F32),
            vmem((layers, nt, 8, tokens), F32),
            vmem((layers, nt, 16, tokens), F32),
            vmem((layers, 32, ch), BF16),
            vmem((layers, 32, ch), BF16),
            vmem((tokens + 32, ch), F32),
            vmem((7, tokens + 24, ch), F32),
            vmem((tokens, ch), F32),
            vmem((tokens, ch), BF16),
            vmem((layers, nt, tokens, ch), BF16),
            vmem((layers, nt, tokens, ch), BF16),
            vmem((layers, 6, tokens, ch), BF16),
            vmem((layers, 6, tokens, ch), BF16),
            dma((layers, 3)),
            dma((layers, 3, 2, 2)),
            dma((layers, 3, 2, half)),
            dma((layers, ns - 1)),
            dma((layers, ns - 1)),
            dma((layers, 14)),
            dma((layers, 2 * nt)),
            dma((layers, 2, nt - 1)),
            dma((layers, 2, nt - 1)),
            dma((layers,)),
            dma((layers,)),
            dma((layers, nt)),
            dma((layers, nt)),
            dma((layers, 6)),
            dma((layers, 6)),
        ]
        v, a = pl.BlockSpec(memory_space=pltpu.VMEM), pl.BlockSpec(memory_space=pl.ANY)
        return pl.pallas_call(
            functools.partial(kernel, sizes),
            out_shape=jax.ShapeDtypeStruct(hidden_in.shape, hidden_in.dtype),
            in_specs=[v, v, a, a, v, v, v, a],
            out_specs=v,
            scratch_shapes=scratch,
            name="layers",
            compiler_params=pltpu.CompilerParams(
                collective_id=0, has_side_effects=True, vmem_limit_bytes=60 * 2**20
            ),
        )(hidden_in, in_gain, w_value, w_gate, conv_taps, norm_gain, norm_shift, w_out)

    placed = (
        P(("grp", "sp"), "tp"),
        P(None, "tp"),
        P(None, "sp", "tp"),
        P(None, "sp", "tp"),
        P(None, None, "tp"),
        P(None, "tp"),
        P(None, "tp"),
        P(None, "tp", "sp"),
    )
    return jax.shard_map(
        shards, mesh=mesh, in_specs=placed, out_specs=P(("grp", "sp"), "tp"), check_vma=False
    )
```

time: 421 us -> 171 us (0.41)
  waiting for transfers between devices: 279 us -> 0 us
  Pallas kernels: 0 us -> 168 us
  starting transfers between devices: 75.8 us -> 0 us
  matrix products: 19.9 us -> 0 us
  between operations: 13.8 us -> 0.01 us
  blocking collectives: 9.85 us -> 0 us
  local copies, waits for them, and re-layouts: 12.2 us -> 3.24 us
  other arithmetic: 8.91 us -> 0 us
    pallas_call x0 -> x1, Pallas kernels: none -> 168 us  [shards(): pl.pallas_call(functools.partial(kernel, sizes), out_shape=jax.ShapeDtype...]
    all_gather x4 -> x0, waiting for transfers between devices: 124 us -> none  [the longest x2 66.9 us: shards(): lax.all_gather(w_out[layer_idx], 'sp', axis=1, tiled=True)]
    reduce_scatter x2 -> x0, waiting for transfers between devices: 93 us -> none  [shards(): lax.psum_scatter(partial_value.astype(jnp.bfloat16), 'tp', scatter_dimens...]
    all_to_all x7 -> x0, starting transfers between devices: 71 us -> none  [from_everyone(): lax.all_to_all(jnp.broadcast_to(x[None], (size, *x.shape)), axis, 0, 0, t...]
    all_to_all x7 -> x0, waiting for transfers between devices: 59.2 us -> none  [from_everyone(): lax.all_to_all(jnp.broadcast_to(x[None], (size, *x.shape)), axis, 0, 0, t...]
    dot_general x6 -> x0, matrix products: 16.3 us -> none  [the longest x2 8.62 us: shards(): jnp.dot(mixed_out, lax.all_gather(w_out[layer_idx], 'sp', axis=1, tiled=T...]
    all_to_all x1 -> x0, blocking collectives: 9.85 us -> none  [from_everyone(): lax.all_to_all(jnp.broadcast_to(x[None], (size, *x.shape)), axis, 0, 0, t...]
    broadcast_in_dim x10 -> x0, local copies, waits for them, and re-layouts: 6.96 us -> none  [the longest x8 6.93 us: from_everyone(): jnp.broadcast_to(x[None], (size, *x.shape))]
  transfers between devices with their start and end apart: 15 -> 0, of which waited for: 14 -> 0; matrix products, arithmetic and copies ran while one was open for 6% -> 0% of each run, Pallas kernels for 0% -> 0%
where the time goes in v1:
time: 171 us
  Pallas kernels  168 us (98%)
  local copies, waits for them, and re-layouts  3.24 us (2%)
    pallas_call x1, Pallas kernels, shards(): pl.pallas_call(functools.partial(kernel, sizes), out_shape=jax.ShapeDtype...  168 us

profile of v1, /device:TPU:33, one launch (start us, length us, event | category | flops | bytes accessed | tf_op | source)
XLA Modules:
  0.0 171.1 jit_solution(5769246216940775230)
XLA Ops:
  0.0 1.5 copy.9.taps
  1.5 167.9 %layers.1 = bf16[384,512]{1,0:T(8,128)(2,1)} custom-call(bf16[384,512]{1,0:T(8,128)(2,1)} %hidden.1, f32[2,512]{1,0:T(2,128)} %in_gain.1, bf16[2,256,256]{2,1,0:T(8,128)(2,1)} %w_value.1, bf16[2,256,256]{2,1,0:T(8,128)(2,1)} %w_gate.1, f32[2,31,256]{2,1,0:T(8,128)} %copy.9.taps, f32[2,256]{1,0:T(2,128)} %norm_gain.1, f32[2,256]{1,0:T(2,128)} %norm_shift.1, ...), custom_call_target="tpu_custom_call" | custom-call | tf_op jit(solution)/shard_map/layers/pallas_call | solution.py:537
  169.4 1.8 %copy.11 = bf16[384,512]{1,0:T(8,128)(2,1)} copy(bf16[384,512]{1,0:T(8,128)(2,1)} %layers.1) | data formatting | bytes 786432

commit v2 on v1

v2 whole, which is shorter than its diff:
```python
import functools

import jax
import jax.numpy as jnp
from jax import lax
from jax.experimental import pallas as pl
from jax.experimental.pallas import tpu as pltpu
from jax.sharding import PartitionSpec as P

MESH = pl.DeviceIdType.MESH
EPS = 1e-06
F32 = jnp.float32
BF16 = jnp.bfloat16
RIGHT, LEFT = 1, -1


def mm(a, b):
    return jnp.dot(a, b, preferred_element_type=F32)


def both(col):
    return jnp.concatenate([col, col], axis=1)


def kernel(
    sizes,
    hidden,
    in_gain,
    w_value,
    w_gate,
    taps,
    norm_gain,
    norm_shift,
    w_out,
    out,
    start,
    wbuf,
    xg,
    cur,
    acc_v,
    acc_g,
    col_a,
    col_b,
    rstat,
    cstat,
    halo_out,
    halo_in,
    ext,
    shifted,
    conved,
    mixed,
    p_out,
    p_in,
    c_out,
    c_in,
    local_sem,
    z_send,
    z_recv,
    y_send,
    y_recv,
    x_send,
    x_recv,
    s_send,
    s_recv,
    h_send,
    h_recv,
    p_send,
    p_recv,
    c_send,
    c_recv,
):
    groups, ns, nt = sizes
    layers = w_value.shape[0]
    rows_w, ch = w_value.shape[1], w_value.shape[2]
    tokens = hidden.shape[0]
    n_taps = taps.shape[0]
    nx = nt // 2
    half = ns // 2
    channels = ch * nt
    features = hidden.shape[1] * nt
    z = lax.axis_index("sp")
    t = lax.axis_index("tp")
    paired = groups % 2 == 0
    x, c = t // 2, lax.rem(t, 2)

    def chip(dx, core):
        return 2 * lax.rem(x + dx + nx, nx) + core

    t_right, t_left, t_opp, t_mate = chip(1, c), chip(-1, c), chip(2, c), 2 * x + (1 - c)

    if paired:
        y = lax.axis_index("grp")
        par = lax.rem(y, 2)
        y_mate = y + 1 - 2 * par
        lone = 80
        ring_rows = rows_w - lone
        ring_base = par * lone
        y_out_at = pl.ds(pl.multiple_of(par * ring_rows, 16), lone)
        y_in_at = pl.ds(pl.multiple_of((1 - par) * ring_rows, 16), lone)
    else:
        ring_rows, ring_base = rows_w, 0

    def zc(offset):
        return lax.rem(z + offset + 2 * ns, ns)

    def remote(src, dst, ssem, rsem, **where):
        return pltpu.make_async_remote_copy(
            src_ref=src, dst_ref=dst, send_sem=ssem, recv_sem=rsem, device_id=where, device_id_type=MESH
        )

    cut = 96
    pieces = ((0, 0, ring_rows), (1, 0, ring_rows), (2, 0, cut), (2, cut, ring_rows - cut))
    early, late = (0, 1), (2, 3)

    def ring_part(l, chunk, p):
        sub, at, rows = pieces[p]
        return wbuf.at[l, chunk, sub, pl.ds(pl.multiple_of(ring_base + at, 16), rows), :]

    def z_copy(l, p, d, s):
        at, way = ring_part(l, zc(-d * (s - 1)), p), 0 if d == RIGHT else 1
        return remote(at, at, z_send.at[l], z_recv.at[l, p, way, s - 1], sp=zc(d))

    def z_arrival(l, p, d, s):
        at, way = ring_part(l, zc(-d * s), p), 0 if d == RIGHT else 1
        return remote(at, at, z_send.at[l], z_recv.at[l, p, way, s - 1], sp=zc(d))

    def active(l, p, d, s):
        if s < half:
            return True
        return s == half and d == (RIGHT, LEFT, RIGHT, LEFT)[p]

    bulk = half - 2

    def y_place(kind, d, s):
        if kind == 1:
            return 4
        if s <= bulk:
            return 0
        return 3 if s == half else (1 if d == RIGHT else 2)

    def y_copy(l, kind, d, s, rows):
        chunk = zc(-d * s)
        at = wbuf.at[l, chunk, pl.ds(0, 2), rows, :] if kind == 0 else wbuf.at[l, chunk, 2, rows, :]
        return remote(at, at, y_send.at[l], y_recv.at[l, y_place(kind, d, s)], grp=y_mate)

    def hop_ways(s):
        return (RIGHT, LEFT) if 0 < s < half else (RIGHT,)

    def z_first(l, which):
        for p in which:
            for d in (RIGHT, LEFT):
                if active(l, p, d, 1):
                    z_copy(l, p, d, 1).start()

    def serve(l, kind, s):
        for p in (early, late)[kind]:
            for d in (RIGHT, LEFT):
                if not active(l, p, d, s):
                    continue
                z_arrival(l, p, d, s).wait_recv()
                if active(l, p, d, s + 1):
                    z_copy(l, p, d, s + 1).start()
        if paired:
            for d in hop_ways(s):
                y_copy(l, kind, d, s, y_out_at).start()

    def z_drain(l):
        part = wbuf.at[l, pl.ds(0, ns - 1), :, pl.ds(0, ring_rows), :]
        pltpu.make_async_copy(part, part, z_send.at[l]).wait()

    def y_wait(l, kind, s):
        if not paired or s == 0:
            return
        if kind == 1:
            part = wbuf.at[l, pl.ds(0, ns - 1), 2, pl.ds(0, lone), :]
            pltpu.make_async_copy(part, part, y_recv.at[l, 4]).wait()
        elif s == bulk:
            part = wbuf.at[l, pl.ds(0, 2 * bulk), pl.ds(0, 2), pl.ds(0, lone), :]
            pltpu.make_async_copy(part, part, y_recv.at[l, 0]).wait()
        elif s > bulk:
            for d in hop_ways(s):
                y_copy(l, 0, d, s, y_in_at).wait_recv()

    def y_drain(l):
        if paired:
            part = wbuf.at[l, pl.ds(0, ns - 1), :, pl.ds(0, lone), :]
            pltpu.make_async_copy(part, part, y_send.at[l]).wait()

    def hop_chunks(s):
        if s == 0 or s == half:
            return [zc(s)]
        return [zc(-s), zc(s)]

    from_left, from_right, from_far, from_mate = 0, 2, 4, 6

    def x_copy(l, chunk, place, to):
        at = xg.at[l, chunk]
        return remote(at, at, x_send.at[l], x_recv.at[l, place], tp=to)

    def x_begin(l):
        a, b = 2 * t, 2 * t + 1
        x_copy(l, a, from_left, t_right).start()
        x_copy(l, b, from_right + 1, t_left).start()
        x_copy(l, b, from_left + 1, t_right).start()
        x_copy(l, a, from_right, t_left).start()
        x_copy(l, a, from_mate, t_mate).start()
        x_copy(l, b, from_mate, t_mate).start()

    def x_share(l, chunk, place):
        x_copy(l, chunk, place, t_mate).wait_recv()
        x_copy(l, chunk, from_mate, t_mate).start()

    def x_near(l):
        a, b = 2 * t_left, 2 * t_right + 1
        x_copy(l, a, from_left, t_mate).wait_recv()
        x_copy(l, a, from_far, t_right).start()
        x_copy(l, a, from_mate, t_mate).start()
        x_copy(l, b, from_right + 1, t_mate).wait_recv()
        x_copy(l, b, from_far + 1, t_left).start()
        x_copy(l, b, from_mate, t_mate).start()

    def x_rest(l):
        x_share(l, 2 * t_left + 1, from_left + 1)
        x_share(l, 2 * t_right, from_right)

    def x_far(l):
        x_share(l, 2 * t_opp, from_far)
        x_share(l, 2 * t_opp + 1, from_far + 1)

    def x_end(l):
        part = xg.at[l, pl.ds(0, nt)]
        pltpu.make_async_copy(part, part, x_recv.at[l, from_mate]).wait()

    def x_drain(l):
        part = xg.at[l, pl.ds(0, 14)]
        pltpu.make_async_copy(part, part, x_send.at[l]).wait()

    def stat_start(buf, l, kind):
        for j in range(1, nt):
            at = buf.at[l, t]
            remote(at, at, s_send.at[l, kind], s_recv.at[l, kind], tp=lax.rem(t + j, nt)).start()

    def stat_wait(buf, l, sem):
        part = buf.at[l, pl.ds(0, nt - 1)]
        pltpu.make_async_copy(part, part, sem).wait()

    groups_of = tokens // 128

    def to_lanes(column):
        wide = jnp.broadcast_to(column, (tokens, 128)).T[:8]
        row = lax.broadcasted_iota(jnp.int32, (8, 128), 0)
        tile = wide[:, :128]
        for i in range(1, groups_of):
            tile = jnp.where(row == i, wide[:, i * 128 : (i + 1) * 128], tile)
        return tile

    def to_column(tile):
        parts = [jnp.broadcast_to(tile[i : i + 1], (128, 128)).T for i in range(groups_of)]
        return jnp.concatenate(parts, axis=0)

    def prepare(l):
        value = cur[...]
        squares = jnp.sum(value * value, axis=1, keepdims=True)
        rstat[l, t] = to_lanes(squares)
        scaled = (value * in_gain[l : l + 1, :]).astype(BF16)
        xg[l, 2 * t] = scaled[:, : scaled.shape[1] // 2]
        xg[l, 2 * t + 1] = scaled[:, scaled.shape[1] // 2 :]

    def accumulate(l, chunks, first):
        for sub, acc in ((0, acc_v), (1, acc_g)):
            total = None if first else acc[...]
            for chunk in chunks:
                part = mm(xg[l, chunk], wbuf[l, chunk, sub])
                total = part if total is None else total + part
            acc[...] = total

    block = 96

    def over_rows(body):
        def step(i, carry):
            body(pl.multiple_of(i * block, block))
            return carry

        lax.fori_loop(0, tokens // block, step, 0)

    def halo_copy(l):
        return remote(halo_out.at[l], halo_in.at[l], h_send.at[l], h_recv.at[l], sp=zc(1))

    reach = halo_out.shape[1]

    def gate(l):
        stat_wait(rstat, l, s_recv.at[l, 0])
        total = rstat[l, 0]
        for j in range(1, nt):
            total = total + rstat[l, j]
        col_a[...] = to_column(lax.rsqrt(total / features + EPS))

        def body(at):
            rows = pl.ds(at, block)
            scale = both(col_a[rows, :])
            value = acc_v[rows, :] * scale
            gated = value * jax.nn.sigmoid(acc_g[rows, :] * scale)
            ext[pl.ds(pl.multiple_of(at + reach, 32), block), :] = gated.astype(BF16).astype(F32)

        over_rows(body)
        halo_out[l] = ext[tokens : tokens + reach, :].astype(BF16)
        halo_copy(l).start()

    small = 32

    def conv_rows(l, lo, hi):
        offset = reach - (n_taps - 1)

        def step(i, carry):
            at = pl.multiple_of(i * small, small)
            total = jnp.zeros((small, ch), F32)
            for k in range(n_taps):
                a, b = ((k + offset) // 8) * 8, (k + offset) % 8
                rows = pl.ds(pl.multiple_of(at + a, 8), small)
                window = ext[rows, :] if b == 0 else shifted[b - 1, rows, :]
                total = total + taps[k, l : l + 1, :] * window
            conved[pl.ds(at, small), :] = total
            return carry

        lax.fori_loop(lo, hi, step, 0)

    def conv_body(l):
        span = shifted.shape[1]
        for b in range(1, 8):
            shifted[b - 1, reach:, :] = ext[reach + b : span + b, :]
        conv_rows(l, 1, tokens // small)

    def conv_head(l):
        halo_copy(l).wait_recv()
        before = halo_in[l].astype(F32)
        ext[:reach, :] = jnp.where(z > 0, before, jnp.zeros_like(before))
        for b in range(1, 8):
            shifted[b - 1, :reach, :] = ext[b : reach + b, :]
        conv_rows(l, 0, 1)
        value = conved[...]
        sums = jnp.sum(value, axis=1, keepdims=True)
        spread = value - sums / ch
        cstat[l, t, 0] = to_lanes(sums)
        cstat[l, t, 1] = to_lanes(jnp.sum(spread * spread, axis=1, keepdims=True))
        stat_start(cstat, l, 1)

    def normalize(l):
        stat_wait(cstat, l, s_recv.at[l, 1])
        total = cstat[l, 0, 0]
        for j in range(1, nt):
            total = total + cstat[l, j, 0]
        mean = total / channels
        spread = jnp.zeros_like(mean)
        for j in range(nt):
            away = cstat[l, j, 0] / ch - mean
            spread = spread + (cstat[l, j, 1] + ch * (away * away))
        col_a[...] = to_column(mean)
        col_b[...] = to_column(lax.rsqrt(spread / channels + EPS))

        def body(at):
            rows = pl.ds(at, block)
            normed = (conved[rows, :] - both(col_a[rows, :])) * both(col_b[rows, :])
            normed = normed * norm_gain[l : l + 1, :] + norm_shift[l : l + 1, :]
            mixed[rows, :] = (normed / (1.0 + jnp.exp(-normed))).astype(BF16)

        over_rows(body)

    def project(l, dx, core, h):
        return mm(mixed[...], wbuf[l, 2 * chip(dx, core) + h, 2])

    def p_copy(l, q):
        return remote(p_out.at[l, q], p_in.at[l, q], p_send.at[l], p_recv.at[l, q], tp=t_mate)

    def c_copy(l, slot):
        to = t_right if slot in (0, 2, 3) else t_left
        return remote(c_out.at[l, slot], c_in.at[l, slot], c_send.at[l], c_recv.at[l, slot], tp=to)

    def give(l, dx, h):
        q = 2 * dx + h
        p_out[l, q] = project(l, dx, 1 - c, h).astype(BF16)
        p_copy(l, q).start()

    def pass_on(l, dx, h, slot, extra=None):
        q = 2 * dx + h
        total = project(l, dx, c, h)
        p_copy(l, q).wait_recv()
        total = total + p_in[l, q].astype(F32)
        if extra is not None:
            c_copy(l, extra).wait_recv()
            total = total + c_in[l, extra].astype(F32)
        c_out[l, slot] = total.astype(BF16)
        c_copy(l, slot).start()

    def settle(l, h, last):
        total = project(l, 0, c, h)
        p_copy(l, h).wait_recv()
        total = total + p_in[l, h].astype(F32)
        for slot in (2 + h, 4 + h):
            c_copy(l, slot).wait_recv()
            total = total + c_in[l, slot].astype(F32)
        cols = slice(h * ch, (h + 1) * ch)
        new = (cur[:, cols] + total).astype(BF16)
        if last:
            out[:, cols] = new
        else:
            cur[:, cols] = new.astype(F32)

    barrier = pltpu.get_barrier_semaphore()
    greeted = [{"tp": lax.rem(t + j, nt)} for j in range(1, nt)]
    greeted += [{"sp": zc(1)}, {"sp": zc(-1)}]
    if paired:
        greeted += [{"grp": y_mate}]
    for where in greeted:
        pl.semaphore_signal(barrier, inc=1, device_id=where, device_id_type=MESH)

    sources = (w_value, w_gate, w_out)
    load = pltpu.make_async_copy(hidden, start, local_sem.at[layers])
    load.start()
    for l in range(layers):
        for sub in range(3):
            pltpu.make_async_copy(sources[sub].at[l], wbuf.at[l, z, sub], local_sem.at[l]).start()

    def loaded(l):
        part = wbuf.at[l, z]
        pltpu.make_async_copy(part, part, local_sem.at[l]).wait()

    def ring_mm(l, s):
        y_wait(l, 0, s)
        if s == bulk:
            for back in range(1, bulk + 1):
                accumulate(l, hop_chunks(back), False)
        elif s == 0 or s > bulk:
            accumulate(l, hop_chunks(s), s == 0)

    loaded(0)
    pl.semaphore_wait(barrier, len(greeted))
    z_first(0, early)
    load.wait()
    cur[...] = start[...].astype(F32)
    prepare(0)
    x_begin(0)
    stat_start(rstat, 0, 0)
    lags = [3 if l == 0 else 4 for l in range(layers)]

    def step(l, s):
        if s <= half:
            serve(l, 0, s)
        if s > lags[l]:
            serve(l, 1, s - lags[l])
        if s == lags[l]:
            z_first(l, late)

    step(0, 1)
    step(0, 2)
    x_near(0)
    step(0, 3)
    x_rest(0)
    x_far(0)
    step(0, 4)
    x_end(0)
    ring_mm(0, 0)
    for s in range(5, half + 1):
        step(0, s)
        ring_mm(0, s - 1)
    ring_mm(0, half)

    for l in range(layers):
        final = l == layers - 1
        n = l + 1

        def more(s):
            if not final:
                step(n, s)

        gate(l)
        rest = list(range(half + 1, half + lags[l] + 1))
        step(l, rest[0])
        conv_body(l)
        step(l, rest[1])
        if not final:
            loaded(n)
            z_first(n, early)
        conv_head(l)
        for s in rest[2:]:
            step(l, s)
        normalize(l)
        more(1)
        y_wait(l, 1, half)
        give(l, 2, 0)
        give(l, 2, 1)
        give(l, 1, 1)
        pass_on(l, 2, 0, 0)
        pass_on(l, 2, 1, 1)
        give(l, 3, 0)
        pass_on(l, 1, 1, 3)
        give(l, 1, 0)
        pass_on(l, 3, 0, 4)
        give(l, 3, 1)
        more(2)
        give(l, 0, 0)
        give(l, 0, 1)
        more(3)
        pass_on(l, 1, 0, 2, 0)
        pass_on(l, 3, 1, 5, 1)
        more(4)
        settle(l, 0, final)
        settle(l, 1, final)
        if not final:
            prepare(n)
            x_begin(n)
            stat_start(rstat, n, 0)
            step(n, 5)
            x_near(n)
            step(n, 6)
            x_rest(n)
            x_far(n)
            step(n, 7)
            x_end(n)
            for s in range(7):
                ring_mm(n, s)
            step(n, half)
            ring_mm(n, half - 1)
            ring_mm(n, half)

    for l in range(layers):
        z_drain(l)
        y_drain(l)
        x_drain(l)
        stat_wait(rstat, l, s_send.at[l, 0])
        stat_wait(cstat, l, s_send.at[l, 1])
        halo_copy(l).wait_send()
        part = p_out.at[l]
        pltpu.make_async_copy(part, part, p_send.at[l]).wait()
        part = c_out.at[l]
        pltpu.make_async_copy(part, part, c_send.at[l]).wait()


def solution(mesh):
    sizes = (mesh.shape["grp"], mesh.shape["sp"], mesh.shape["tp"])
    groups, ns, nt = sizes

    def shards(hidden_in, in_gain, w_value, w_gate, conv_taps, norm_gain, norm_shift, w_out):
        layers, rows_w, ch = w_value.shape
        tokens = hidden_in.shape[0]
        vmem = pltpu.VMEM
        dma = pltpu.SemaphoreType.DMA
        half = ns // 2
        scratch = [
            vmem(hidden_in.shape, BF16),
            vmem((layers, ns, 3, rows_w, ch), BF16),
            vmem((layers, 2 * nt, tokens, ch), BF16),
            vmem((tokens, 2 * ch), F32),
            vmem((tokens, ch), F32),
            vmem((tokens, ch), F32),
            vmem((tokens, 128), F32),
            vmem((tokens, 128), F32),
            vmem((layers, nt, 8, 128), F32),
            vmem((layers, nt, 2, 8, 128), F32),
            vmem((layers, 32, ch), BF16),
            vmem((layers, 32, ch), BF16),
            vmem((tokens + 32, ch), F32),
            vmem((7, tokens + 24, ch), F32),
            vmem((tokens, ch), F32),
            vmem((tokens, ch), BF16),
            vmem((layers, nt, tokens, ch), BF16),
            vmem((layers, nt, tokens, ch), BF16),
            vmem((layers, 6, tokens, ch), BF16),
            vmem((layers, 6, tokens, ch), BF16),
            dma((layers + 1,)),
            dma((layers,)),
            dma((layers, 4, 2, half)),
            dma((layers,)),
            dma((layers, 5)),
            dma((layers,)),
            dma((layers, 7)),
            dma((layers, 2)),
            dma((layers, 2)),
            dma((layers,)),
            dma((layers,)),
            dma((layers,)),
            dma((layers, nt)),
            dma((layers,)),
            dma((layers, 6)),
        ]
        v, a = pl.BlockSpec(memory_space=pltpu.VMEM), pl.BlockSpec(memory_space=pl.ANY)
        return pl.pallas_call(
            functools.partial(kernel, sizes),
            out_shape=jax.ShapeDtypeStruct(hidden_in.shape, hidden_in.dtype),
            in_specs=[a, v, a, a, v, v, v, a],
            out_specs=v,
            scratch_shapes=scratch,
            name="layers",
            compiler_params=pltpu.CompilerParams(
                collective_id=0, has_side_effects=True, vmem_limit_bytes=60 * 2**20
            ),
        )(hidden_in, in_gain, w_value, w_gate, jnp.transpose(conv_taps, (1, 0, 2)), norm_gain, norm_shift, w_out)

    placed = (
        P(("grp", "sp"), "tp"),
        P(None, "tp"),
        P(None, "sp", "tp"),
        P(None, "sp", "tp"),
        P(None, None, "tp"),
        P(None, "tp"),
        P(None, "tp"),
        P(None, "tp", "sp"),
    )
    return jax.shard_map(
        shards, mesh=mesh, in_specs=placed, out_specs=P(("grp", "sp"), "tp"), check_vma=False
    )
```

time: 171 us -> 162 us (0.947)
  Pallas kernels: 168 us -> 160 us
    pallas_call x1, Pallas kernels: 168 us -> 160 us  [shards(): pl.pallas_call(functools.partial(kernel, sizes), out_shape=jax.ShapeDtype...]
where the time goes in v2:
time: 162 us
  Pallas kernels  160 us (99%)
  local copies, waits for them, and re-layouts  1.77 us (1%)
    pallas_call x1, Pallas kernels, shards(): pl.pallas_call(functools.partial(kernel, sizes), out_shape=jax.ShapeDtype...  160 us

profile of v2, /device:TPU:33, one launch (start us, length us, event | category | flops | bytes accessed | tf_op | source)
XLA Modules:
  0.0 162.2 jit_solution(14091568993670747853)
XLA Ops:
  0.0 160.4 %layers.1 = bf16[384,512]{1,0:T(8,128)(2,1)} custom-call(bf16[384,512]{1,0:T(8,128)(2,1)} %hidden.1, f32[2,512]{1,0:T(2,128)} %in_gain.1, bf16[2,256,256]{2,1,0:T(8,128)(2,1)} %w_value.1, bf16[2,256,256]{2,1,0:T(8,128)(2,1)} %w_gate.1, f32[31,2,256]{2,1,0:T(2,128)} %bitcast.1, f32[2,256]{1,0:T(2,128)} %norm_gain.1, f32[2,256]{1,0:T(2,128)} %norm_shift.1, ...), custom_call_target="tpu_custom_call" | custom-call | tf_op jit(solution)/shard_map/layers/pallas_call | solution.py:586
  160.4 1.8 %copy.10 = bf16[384,512]{1,0:T(8,128)(2,1)} copy(bf16[384,512]{1,0:T(8,128)(2,1)} %layers.1) | data formatting | bytes 786432

commit v3 on v2

--- a/solution.py
+++ b/solution.py
@@ -57,7 +57,10 @@
     z_send,
     z_recv,
     y_send,
-    y_recv,
+    g_send,
+    w_recv,
+    m_send,
+    m_recv,
     x_send,
     x_recv,
     s_send,
@@ -108,137 +111,190 @@
             src_ref=src, dst_ref=dst, send_sem=ssem, recv_sem=rsem, device_id=where, device_id_type=MESH
         )
 
-    cut = 96
-    pieces = ((0, 0, ring_rows), (1, 0, ring_rows), (2, 0, cut), (2, cut, ring_rows - cut))
-    early, late = (0, 1), (2, 3)
-
-    def ring_part(l, chunk, p):
-        sub, at, rows = pieces[p]
-        return wbuf.at[l, chunk, sub, pl.ds(pl.multiple_of(ring_base + at, 16), rows), :]
-
-    def z_copy(l, p, d, s):
-        at, way = ring_part(l, zc(-d * (s - 1)), p), 0 if d == RIGHT else 1
-        return remote(at, at, z_send.at[l], z_recv.at[l, p, way, s - 1], sp=zc(d))
-
-    def z_arrival(l, p, d, s):
-        at, way = ring_part(l, zc(-d * s), p), 0 if d == RIGHT else 1
-        return remote(at, at, z_send.at[l], z_recv.at[l, p, way, s - 1], sp=zc(d))
-
-    def active(l, p, d, s):
+    early, late = (0, 1), (2,)
+    first_core = c == 0
+    second_core = c == 1
+
+    def hand_over(l):
+        return remote(wbuf.at[l, 0, z], wbuf.at[l, 1, z], m_send.at[l], m_recv.at[l], tp=t_mate)
+
+    def ring_part(l, col, chunk, sub):
+        return wbuf.at[l, col, chunk, sub, pl.ds(pl.multiple_of(ring_base, 16), ring_rows), :]
+
+    def z_copy(l, col, sub, d, s):
+        at, way = ring_part(l, col, zc(-d * (s - 1)), sub), 0 if d == RIGHT else 1
+        return remote(at, at, z_send.at[l], z_recv.at[col, sub, way, s % 4], sp=zc(d))
+
+    def z_arrival(l, col, sub, d, s):
+        at, way = ring_part(l, col, zc(-d * s), sub), 0 if d == RIGHT else 1
+        return remote(at, at, z_send.at[l], z_recv.at[col, sub, way, s % 4], sp=zc(d))
+
+    def active(l, sub, d, s):
         if s < half:
             return True
-        return s == half and d == (RIGHT, LEFT, RIGHT, LEFT)[p]
+        return s == half and d == (RIGHT, LEFT, RIGHT if l % 2 == 0 else LEFT)[sub]
 
     bulk = half - 2
 
-    def y_place(kind, d, s):
+    def place(kind, d, s):
         if kind == 1:
             return 4
         if s <= bulk:
             return 0
         return 3 if s == half else (1 if d == RIGHT else 2)
 
-    def y_copy(l, kind, d, s, rows):
+    def give_mate(l, kind, sub, d, s):
         chunk = zc(-d * s)
-        at = wbuf.at[l, chunk, pl.ds(0, 2), rows, :] if kind == 0 else wbuf.at[l, chunk, 2, rows, :]
-        return remote(at, at, y_send.at[l], y_recv.at[l, y_place(kind, d, s)], grp=y_mate)
+        src, dst = ring_part(l, 1, chunk, sub), ring_part(l, 0, chunk, sub)
+        return remote(src, dst, g_send.at[l], w_recv.at[l, place(kind, d, s)], tp=t_mate)
+
+    def y_copy(l, col, kind, d, s, rows):
+        chunk = zc(-d * s)
+        subs = pl.ds(0, 2) if kind == 0 else pl.ds(2, 1)
+        src, dst = wbuf.at[l, col, chunk, subs, rows, :], wbuf.at[l, 0, chunk, subs, rows, :]
+        where = {"grp": y_mate} if col == 0 else {"grp": y_mate, "tp": t_mate}
+        return remote(src, dst, y_send.at[l], w_recv.at[l, place(kind, d, s)], **where)
 
     def hop_ways(s):
         return (RIGHT, LEFT) if 0 < s < half else (RIGHT,)
 
     def z_first(l, which):
-        for p in which:
-            for d in (RIGHT, LEFT):
-                if active(l, p, d, 1):
-                    z_copy(l, p, d, 1).start()
+        @pl.when(second_core)
+        def _():
+            for col in range(2):
+                if col == 1 and which[0] == 0:
+                    hand_over(l).wait_recv()
+                for sub in which:
+                    for d in (RIGHT, LEFT):
+                        z_copy(l, col, sub, d, 1).start()
 
     def serve(l, kind, s):
-        for p in (early, late)[kind]:
-            for d in (RIGHT, LEFT):
-                if not active(l, p, d, s):
-                    continue
-                z_arrival(l, p, d, s).wait_recv()
-                if active(l, p, d, s + 1):
-                    z_copy(l, p, d, s + 1).start()
-        if paired:
-            for d in hop_ways(s):
-                y_copy(l, kind, d, s, y_out_at).start()
-
-    def z_drain(l):
-        part = wbuf.at[l, pl.ds(0, ns - 1), :, pl.ds(0, ring_rows), :]
-        pltpu.make_async_copy(part, part, z_send.at[l]).wait()
-
-    def y_wait(l, kind, s):
-        if not paired or s == 0:
+        subs = (early, late)[kind]
+        for sub in subs:
+            for col in range(2):
+                for d in (RIGHT, LEFT):
+                    if not active(l, sub, d, s):
+                        continue
+                    z_arrival(l, col, sub, d, s).wait_recv()
+                    if active(l, sub, d, s + 1):
+                        z_copy(l, col, sub, d, s + 1).start()
+                    if col == 1:
+                        give_mate(l, kind, sub, d, s).start()
+                    if paired and sub == subs[-1]:
+                        y_copy(l, col, kind, d, s, y_out_at).start()
+
+    def take(l, kind, s, rows):
+        if s == 0:
             return
         if kind == 1:
-            part = wbuf.at[l, pl.ds(0, ns - 1), 2, pl.ds(0, lone), :]
-            pltpu.make_async_copy(part, part, y_recv.at[l, 4]).wait()
+            parts = [(wbuf.at[l, 0, pl.ds(0, ns - 1), 2, pl.ds(0, rows), :], 4)]
+        elif s < bulk:
+            return
         elif s == bulk:
-            part = wbuf.at[l, pl.ds(0, 2 * bulk), pl.ds(0, 2), pl.ds(0, lone), :]
-            pltpu.make_async_copy(part, part, y_recv.at[l, 0]).wait()
-        elif s > bulk:
-            for d in hop_ways(s):
-                y_copy(l, 0, d, s, y_in_at).wait_recv()
-
-    def y_drain(l):
+            parts = [(wbuf.at[l, 0, pl.ds(0, 2 * bulk), pl.ds(0, 2), pl.ds(0, rows), :], 0)]
+        else:
+            parts = [(wbuf.at[l, 0, 0, pl.ds(0, 2), pl.ds(0, rows), :], place(0, d, s)) for d in hop_ways(s)]
+        for part, sem in parts:
+            pltpu.make_async_copy(part, part, w_recv.at[l, sem]).wait()
+
+    def w_wait(l, kind, s):
         if paired:
-            part = wbuf.at[l, pl.ds(0, ns - 1), :, pl.ds(0, lone), :]
-            pltpu.make_async_copy(part, part, y_send.at[l]).wait()
+
+            @pl.when(second_core)
+            def _():
+                take(l, kind, s, lone)
+
+        @pl.when(first_core)
+        def _():
+            take(l, kind, s, rows_w)
+
+    def w_drain(l):
+        def wait(part, sem):
+            pltpu.make_async_copy(part, part, sem).wait()
+
+        @pl.when(second_core)
+        def _():
+            sent = wbuf.at[l, :, pl.ds(0, ns - 1), :, pl.ds(0, ring_rows), :]
+            wait(sent, z_send.at[l])
+            wait(sent.at[0], g_send.at[l])
+            if paired:
+                wait(wbuf.at[l, :, pl.ds(0, ns - 1), :, pl.ds(0, lone), :], y_send.at[l])
+
+        @pl.when(first_core)
+        def _():
+            hand_over(l).wait_send()
 
     def hop_chunks(s):
         if s == 0 or s == half:
             return [zc(s)]
         return [zc(-s), zc(s)]
 
-    from_left, from_right, from_far, from_mate = 0, 2, 4, 6
-
-    def x_copy(l, chunk, place, to):
+    from_left, from_right, from_far, from_mate = 0, 4, 8, 12
+
+    def x_copy(l, chunk, where, to):
         at = xg.at[l, chunk]
-        return remote(at, at, x_send.at[l], x_recv.at[l, place], tp=to)
+        return remote(at, at, x_send.at[l], x_recv.at[where], tp=to)
+
+    def x_two(l, owner):
+        own = 2 * owner
+        part = xg.at[l, pl.ds(own, 2)]
+        return remote(part, part, x_send.at[l], x_recv.at[from_mate], tp=t_mate)
+
+    def x_out(l, owner, k):
+        a, b = 2 * owner, 2 * owner + 1
+        x_copy(l, a, from_left + k, t_right).start()
+        x_copy(l, b, from_right + k + 1, t_left).start()
+        x_copy(l, b, from_left + k + 1, t_right).start()
+        x_copy(l, a, from_right + k, t_left).start()
 
     def x_begin(l):
-        a, b = 2 * t, 2 * t + 1
-        x_copy(l, a, from_left, t_right).start()
-        x_copy(l, b, from_right + 1, t_left).start()
-        x_copy(l, b, from_left + 1, t_right).start()
-        x_copy(l, a, from_right, t_left).start()
-        x_copy(l, a, from_mate, t_mate).start()
-        x_copy(l, b, from_mate, t_mate).start()
-
-    def x_share(l, chunk, place):
-        x_copy(l, chunk, place, t_mate).wait_recv()
+        x_two(l, t).start()
+
+        @pl.when(first_core)
+        def _():
+            x_out(l, t, 0)
+            x_two(l, t_mate).wait_recv()
+            x_out(l, t_mate, 2)
+
+    def x_share(l, chunk, where):
+        x_copy(l, chunk, where, t_mate).wait_recv()
         x_copy(l, chunk, from_mate, t_mate).start()
 
-    def x_near(l):
-        a, b = 2 * t_left, 2 * t_right + 1
-        x_copy(l, a, from_left, t_mate).wait_recv()
-        x_copy(l, a, from_far, t_right).start()
-        x_copy(l, a, from_mate, t_mate).start()
-        x_copy(l, b, from_right + 1, t_mate).wait_recv()
-        x_copy(l, b, from_far + 1, t_left).start()
-        x_copy(l, b, from_mate, t_mate).start()
-
-    def x_rest(l):
-        x_share(l, 2 * t_left + 1, from_left + 1)
-        x_share(l, 2 * t_right, from_right)
-
-    def x_far(l):
-        x_share(l, 2 * t_opp, from_far)
-        x_share(l, 2 * t_opp + 1, from_far + 1)
+    def x_gather(l):
+        for k in (0, 2):
+            core = k // 2
+            a, b = 2 * chip(-1, core), 2 * chip(1, core) + 1
+            x_copy(l, a, from_left + k, t_mate).wait_recv()
+            x_copy(l, a, from_far + k, t_right).start()
+            x_copy(l, a, from_mate, t_mate).start()
+            x_copy(l, b, from_right + k + 1, t_mate).wait_recv()
+            x_copy(l, b, from_far + k + 1, t_left).start()
+            x_copy(l, b, from_mate, t_mate).start()
+            x_share(l, 2 * chip(-1, core) + 1, from_left + k + 1)
+            x_share(l, 2 * chip(1, core), from_right + k)
+        for k in (0, 2):
+            x_share(l, 2 * chip(2, k // 2), from_far + k)
+            x_share(l, 2 * chip(2, k // 2) + 1, from_far + k + 1)
 
     def x_end(l):
-        part = xg.at[l, pl.ds(0, nt)]
-        pltpu.make_async_copy(part, part, x_recv.at[l, from_mate]).wait()
+        part = xg.at[l, pl.ds(0, 2 * nt - 2)]
+        pltpu.make_async_copy(part, part, x_recv.at[from_mate]).wait()
 
     def x_drain(l):
-        part = xg.at[l, pl.ds(0, 14)]
-        pltpu.make_async_copy(part, part, x_send.at[l]).wait()
+        @pl.when(second_core)
+        def _():
+            x_two(l, t).wait_send()
+
+        @pl.when(first_core)
+        def _():
+            for count in (2 * nt - 2, 12):
+                part = xg.at[l, pl.ds(0, count)]
+                pltpu.make_async_copy(part, part, x_send.at[l]).wait()
 
     def stat_start(buf, l, kind):
         for j in range(1, nt):
             at = buf.at[l, t]
-            remote(at, at, s_send.at[l, kind], s_recv.at[l, kind], tp=lax.rem(t + j, nt)).start()
+            remote(at, at, s_send.at[l, kind], s_recv.at[kind], tp=lax.rem(t + j, nt)).start()
 
     def stat_wait(buf, l, sem):
         part = buf.at[l, pl.ds(0, nt - 1)]
@@ -270,7 +326,7 @@
         for sub, acc in ((0, acc_v), (1, acc_g)):
             total = None if first else acc[...]
             for chunk in chunks:
-                part = mm(xg[l, chunk], wbuf[l, chunk, sub])
+                part = mm(xg[l, chunk], wbuf[l, 0, chunk, sub])
                 total = part if total is None else total + part
             acc[...] = total
 
@@ -289,7 +345,7 @@
     reach = halo_out.shape[1]
 
     def gate(l):
-        stat_wait(rstat, l, s_recv.at[l, 0])
+        stat_wait(rstat, l, s_recv.at[0])
         total = rstat[l, 0]
         for j in range(1, nt):
             total = total + rstat[l, j]
@@ -345,7 +401,7 @@
         stat_start(cstat, l, 1)
 
     def normalize(l):
-        stat_wait(cstat, l, s_recv.at[l, 1])
+        stat_wait(cstat, l, s_recv.at[1])
         total = cstat[l, 0, 0]
         for j in range(1, nt):
             total = total + cstat[l, j, 0]
@@ -366,14 +422,14 @@
         over_rows(body)
 
     def project(l, dx, core, h):
-        return mm(mixed[...], wbuf[l, 2 * chip(dx, core) + h, 2])
+        return mm(mixed[...], wbuf[l, 0, 2 * chip(dx, core) + h, 2])
 
     def p_copy(l, q):
-        return remote(p_out.at[l, q], p_in.at[l, q], p_send.at[l], p_recv.at[l, q], tp=t_mate)
+        return remote(p_out.at[l, q], p_in.at[l, q], p_send.at[l], p_recv.at[q], tp=t_mate)
 
     def c_copy(l, slot):
         to = t_right if slot in (0, 2, 3) else t_left
-        return remote(c_out.at[l, slot], c_in.at[l, slot], c_send.at[l], c_recv.at[l, slot], tp=to)
+        return remote(c_out.at[l, slot], c_in.at[l, slot], c_send.at[l], c_recv.at[slot], tp=to)
 
     def give(l, dx, h):
         q = 2 * dx + h
@@ -409,7 +465,7 @@
     greeted = [{"tp": lax.rem(t + j, nt)} for j in range(1, nt)]
     greeted += [{"sp": zc(1)}, {"sp": zc(-1)}]
     if paired:
-        greeted += [{"grp": y_mate}]
+        greeted += [{"grp": y_mate}, {"grp": y_mate, "tp": t_mate}]
     for where in greeted:
         pl.semaphore_signal(barrier, inc=1, device_id=where, device_id_type=MESH)
 
@@ -418,14 +474,14 @@
     load.start()
     for l in range(layers):
         for sub in range(3):
-            pltpu.make_async_copy(sources[sub].at[l], wbuf.at[l, z, sub], local_sem.at[l]).start()
+            pltpu.make_async_copy(sources[sub].at[l], wbuf.at[l, 0, z, sub], local_sem.at[l]).start()
 
     def loaded(l):
-        part = wbuf.at[l, z]
+        part = wbuf.at[l, 0, z]
         pltpu.make_async_copy(part, part, local_sem.at[l]).wait()
 
     def ring_mm(l, s):
-        y_wait(l, 0, s)
+        w_wait(l, 0, s)
         if s == bulk:
             for back in range(1, bulk + 1):
                 accumulate(l, hop_chunks(back), False)
@@ -434,34 +490,58 @@
 
     loaded(0)
     pl.semaphore_wait(barrier, len(greeted))
+
+    @pl.when(first_core)
+    def _():
+        hand_over(0).start()
+
     z_first(0, early)
     load.wait()
     cur[...] = start[...].astype(F32)
     prepare(0)
     x_begin(0)
     stat_start(rstat, 0, 0)
-    lags = [3 if l == 0 else 4 for l in range(layers)]
+
+    @pl.when(first_core)
+    def _():
+        for l in range(1, layers):
+            loaded(l)
+            hand_over(l).start()
+
+    lags = [3 for l in range(layers)]
 
     def step(l, s):
         if s <= half:
             serve(l, 0, s)
         if s > lags[l]:
             serve(l, 1, s - lags[l])
-        if s == lags[l]:
-            z_first(l, late)
-
-    step(0, 1)
-    step(0, 2)
-    x_near(0)
-    step(0, 3)
-    x_rest(0)
-    x_far(0)
-    step(0, 4)
-    x_end(0)
+
+    def steps(l, first, end):
+        @pl.when(second_core)
+        def _():
+            for s in range(first, end):
+                step(l, s)
+
+        for s in range(first, end):
+            if s == lags[l]:
+                z_first(l, late)
+
+    steps(0, 1, 4)
+    steps(0, 4, 5)
+
+    @pl.when(first_core)
+    def _():
+        x_gather(0)
+
+    @pl.when(second_core)
+    def _():
+        x_end(0)
+
     ring_mm(0, 0)
     for s in range(5, half + 1):
-        step(0, s)
+        steps(0, s, s + 1)
         ring_mm(0, s - 1)
+    steps(0, half + 1, half + 2)
     ring_mm(0, half)
 
     for l in range(layers):
@@ -470,22 +550,24 @@
 
         def more(s):
             if not final:
-                step(n, s)
+                steps(n, s, s + 1)
 
         gate(l)
-        rest = list(range(half + 1, half + lags[l] + 1))
-        step(l, rest[0])
+        rest = half + 2
         conv_body(l)
-        step(l, rest[1])
+        steps(l, rest, rest + 1)
         if not final:
-            loaded(n)
+
+            @pl.when(second_core)
+            def _():
+                loaded(n)
+
             z_first(n, early)
         conv_head(l)
-        for s in rest[2:]:
-            step(l, s)
+        steps(l, rest + 1, half + lags[l] + 1)
         normalize(l)
         more(1)
-        y_wait(l, 1, half)
+        w_wait(l, 1, half)
         give(l, 2, 0)
         give(l, 2, 1)
         give(l, 1, 1)
@@ -496,12 +578,12 @@
         give(l, 1, 0)
         pass_on(l, 3, 0, 4)
         give(l, 3, 1)
-        more(2)
         give(l, 0, 0)
         give(l, 0, 1)
-        more(3)
+        more(2)
         pass_on(l, 1, 0, 2, 0)
         pass_on(l, 3, 1, 5, 1)
+        more(3)
         more(4)
         settle(l, 0, final)
         settle(l, 1, final)
@@ -509,22 +591,25 @@
             prepare(n)
             x_begin(n)
             stat_start(rstat, n, 0)
-            step(n, 5)
-            x_near(n)
-            step(n, 6)
-            x_rest(n)
-            x_far(n)
-            step(n, 7)
-            x_end(n)
+            steps(n, 5, 8)
+
+            @pl.when(first_core)
+            def _():
+                x_gather(n)
+
+            @pl.when(second_core)
+            def _():
+                x_end(n)
+
             for s in range(7):
                 ring_mm(n, s)
-            step(n, half)
+            steps(n, half, half + 1)
             ring_mm(n, half - 1)
+            steps(n, half + 1, half + 2)
             ring_mm(n, half)
 
     for l in range(layers):
-        z_drain(l)
-        y_drain(l)
+        w_drain(l)
         x_drain(l)
         stat_wait(rstat, l, s_send.at[l, 0])
         stat_wait(cstat, l, s_send.at[l, 1])
@@ -547,7 +632,7 @@
         half = ns // 2
         scratch = [
             vmem(hidden_in.shape, BF16),
-            vmem((layers, ns, 3, rows_w, ch), BF16),
+            vmem((layers, 2, ns, 3, rows_w, ch), BF16),
             vmem((layers, 2 * nt, tokens, ch), BF16),
             vmem((tokens, 2 * ch), F32),
             vmem((tokens, ch), F32),
@@ -568,19 +653,22 @@
             vmem((layers, 6, tokens, ch), BF16),
             dma((layers + 1,)),
             dma((layers,)),
-            dma((layers, 4, 2, half)),
+            dma((2, 3, 2, 4)),
+            dma((layers,)),
             dma((layers,)),
             dma((layers, 5)),
             dma((layers,)),
-            dma((layers, 7)),
+            dma((layers,)),
+            dma((layers,)),
+            dma((13,)),
             dma((layers, 2)),
-            dma((layers, 2)),
-            dma((layers,)),
-            dma((layers,)),
-            dma((layers,)),
-            dma((layers, nt)),
-            dma((layers,)),
-            dma((layers, 6)),
+            dma((2,)),
+            dma((layers,)),
+            dma((layers,)),
+            dma((layers,)),
+            dma((nt,)),
+            dma((layers,)),
+            dma((6,)),
         ]
         v, a = pl.BlockSpec(memory_space=pltpu.VMEM), pl.BlockSpec(memory_space=pl.ANY)
         return pl.pallas_call(

time: 162 us -> 150 us (0.926)
  Pallas kernels: 160 us -> 148 us
    pallas_call x1, Pallas kernels: 160 us -> 148 us  [shards(): pl.pallas_call(functools.partial(kernel, sizes), out_shape=jax.ShapeDtype...]
where the time goes in v3:
time: 150 us
  Pallas kernels  148 us (99%)
  local copies, waits for them, and re-layouts  1.77 us (1%)
    pallas_call x1, Pallas kernels, shards(): pl.pallas_call(functools.partial(kernel, sizes), out_shape=jax.ShapeDtype...  148 us

profile of v3, /device:TPU:33, one launch (start us, length us, event | category | flops | bytes accessed | tf_op | source)
XLA Modules:
  0.0 150.0 jit_solution(16484027992562003827)
XLA Ops:
  0.0 148.2 %layers.1 = bf16[384,512]{1,0:T(8,128)(2,1)} custom-call(bf16[384,512]{1,0:T(8,128)(2,1)} %hidden.1, f32[2,512]{1,0:T(2,128)} %in_gain.1, bf16[2,256,256]{2,1,0:T(8,128)(2,1)} %w_value.1, bf16[2,256,256]{2,1,0:T(8,128)(2,1)} %w_gate.1, f32[31,2,256]{2,1,0:T(2,128)} %bitcast.1, f32[2,256]{1,0:T(2,128)} %norm_gain.1, f32[2,256]{1,0:T(2,128)} %norm_shift.1, ...), custom_call_target="tpu_custom_call" | custom-call | tf_op jit(solution)/shard_map/layers/pallas_call | solution.py:674
  148.3 1.8 %copy.10 = bf16[384,512]{1,0:T(8,128)(2,1)} copy(bf16[384,512]{1,0:T(8,128)(2,1)} %layers.1) | data formatting | bytes 786432

commit v4 on v3

--- a/solution.py
+++ b/solution.py
@@ -25,14 +25,19 @@
 def kernel(
     sizes,
     hidden,
-    in_gain,
+    in_gain_in,
     w_value,
     w_gate,
+    taps_in,
+    norm_gain_in,
+    norm_shift_in,
+    w_out,
+    out,
+    in_gain,
     taps,
     norm_gain,
     norm_shift,
-    w_out,
-    out,
+    result,
     start,
     wbuf,
     xg,
@@ -54,6 +59,7 @@
     c_out,
     c_in,
     local_sem,
+    out_sem,
     z_send,
     z_recv,
     y_send,
@@ -161,17 +167,20 @@
     def z_first(l, which):
         @pl.when(second_core)
         def _():
-            for col in range(2):
-                if col == 1 and which[0] == 0:
+            first = which[0] == 0
+            if first and l > 0:
+                hand_over(l).wait_recv()
+            for col in (0, 1) if first and l == 0 else (1, 0):
+                if first and l == 0 and col == 1:
                     hand_over(l).wait_recv()
                 for sub in which:
                     for d in (RIGHT, LEFT):
                         z_copy(l, col, sub, d, 1).start()
 
-    def serve(l, kind, s):
+    def serve(l, kind, s, some=None):
         subs = (early, late)[kind]
-        for sub in subs:
-            for col in range(2):
+        for sub in some or subs:
+            for col in (1, 0):
                 for d in (RIGHT, LEFT):
                     if not active(l, sub, d, s):
                         continue
@@ -457,7 +466,8 @@
         cols = slice(h * ch, (h + 1) * ch)
         new = (cur[:, cols] + total).astype(BF16)
         if last:
-            out[:, cols] = new
+            result[h] = new
+            pltpu.make_async_copy(result.at[h], out.at[:, cols], out_sem.at[h]).start()
         else:
             cur[:, cols] = new.astype(F32)
 
@@ -470,11 +480,24 @@
         pl.semaphore_signal(barrier, inc=1, device_id=where, device_id_type=MESH)
 
     sources = (w_value, w_gate, w_out)
-    load = pltpu.make_async_copy(hidden, start, local_sem.at[layers])
-    load.start()
+    loads = [
+        pltpu.make_async_copy(src, dst, local_sem.at[layers + i])
+        for i, (src, dst) in enumerate(
+            (
+                (hidden, start),
+                (in_gain_in, in_gain),
+                (taps_in, taps),
+                (norm_gain_in, norm_gain),
+                (norm_shift_in, norm_shift),
+            )
+        )
+    ]
     for l in range(layers):
         for sub in range(3):
             pltpu.make_async_copy(sources[sub].at[l], wbuf.at[l, 0, z, sub], local_sem.at[l]).start()
+        if l == 0:
+            for load in loads:
+                load.start()
 
     def loaded(l):
         part = wbuf.at[l, 0, z]
@@ -496,7 +519,8 @@
         hand_over(0).start()
 
     z_first(0, early)
-    load.wait()
+    for load in loads:
+        load.wait()
     cur[...] = start[...].astype(F32)
     prepare(0)
     x_begin(0)
@@ -523,7 +547,7 @@
                 step(l, s)
 
         for s in range(first, end):
-            if s == lags[l]:
+            if s == lags[l] and l == 0:
                 z_first(l, late)
 
     steps(0, 1, 4)
@@ -552,6 +576,13 @@
             if not final:
                 steps(n, s, s + 1)
 
+        def part(s, sub):
+            if not final:
+
+                @pl.when(second_core)
+                def _():
+                    serve(n, 0, s, (sub,))
+
         gate(l)
         rest = half + 2
         conv_body(l)
@@ -566,24 +597,29 @@
         conv_head(l)
         steps(l, rest + 1, half + lags[l] + 1)
         normalize(l)
-        more(1)
+        part(1, 0)
         w_wait(l, 1, half)
         give(l, 2, 0)
         give(l, 2, 1)
         give(l, 1, 1)
+        part(1, 1)
         pass_on(l, 2, 0, 0)
         pass_on(l, 2, 1, 1)
         give(l, 3, 0)
         pass_on(l, 1, 1, 3)
+        part(2, 0)
         give(l, 1, 0)
         pass_on(l, 3, 0, 4)
         give(l, 3, 1)
+        part(2, 1)
         give(l, 0, 0)
         give(l, 0, 1)
-        more(2)
+        part(3, 0)
         pass_on(l, 1, 0, 2, 0)
         pass_on(l, 3, 1, 5, 1)
-        more(3)
+        part(3, 1)
+        if not final:
+            z_first(n, late)
         more(4)
         settle(l, 0, final)
         settle(l, 1, final)
@@ -591,7 +627,7 @@
             prepare(n)
             x_begin(n)
             stat_start(rstat, n, 0)
-            steps(n, 5, 8)
+            steps(n, 5, half + 1)
 
             @pl.when(first_core)
             def _():
@@ -603,11 +639,12 @@
 
             for s in range(7):
                 ring_mm(n, s)
-            steps(n, half, half + 1)
             ring_mm(n, half - 1)
             steps(n, half + 1, half + 2)
             ring_mm(n, half)
 
+    for h in range(2):
+        pltpu.make_async_copy(result.at[h], out.at[:, h * ch : (h + 1) * ch], out_sem.at[h]).wait()
     for l in range(layers):
         w_drain(l)
         x_drain(l)
@@ -631,6 +668,11 @@
         dma = pltpu.SemaphoreType.DMA
         half = ns // 2
         scratch = [
+            vmem(in_gain.shape, F32),
+            vmem((conv_taps.shape[1], layers, ch), F32),
+            vmem(norm_gain.shape, F32),
+            vmem(norm_shift.shape, F32),
+            vmem((2, tokens, ch), BF16),
             vmem(hidden_in.shape, BF16),
             vmem((layers, 2, ns, 3, rows_w, ch), BF16),
             vmem((layers, 2 * nt, tokens, ch), BF16),
@@ -651,7 +693,8 @@
             vmem((layers, nt, tokens, ch), BF16),
             vmem((layers, 6, tokens, ch), BF16),
             vmem((layers, 6, tokens, ch), BF16),
-            dma((layers + 1,)),
+            dma((layers + 5,)),
+            dma((2,)),
             dma((layers,)),
             dma((2, 3, 2, 4)),
             dma((layers,)),
@@ -670,12 +713,12 @@
             dma((layers,)),
             dma((6,)),
         ]
-        v, a = pl.BlockSpec(memory_space=pltpu.VMEM), pl.BlockSpec(memory_space=pl.ANY)
+        a = pl.BlockSpec(memory_space=pl.ANY)
         return pl.pallas_call(
             functools.partial(kernel, sizes),
             out_shape=jax.ShapeDtypeStruct(hidden_in.shape, hidden_in.dtype),
-            in_specs=[a, v, a, a, v, v, v, a],
-            out_specs=v,
+            in_specs=[a] * 8,
+            out_specs=a,
             scratch_shapes=scratch,
             name="layers",
             compiler_params=pltpu.CompilerParams(

time: 150 us -> 146 us (0.973)
  Pallas kernels: 148 us -> 144 us
    pallas_call x1, Pallas kernels: 148 us -> 144 us  [shards(): pl.pallas_call(functools.partial(kernel, sizes), out_shape=jax.ShapeDtype...]
where the time goes in v4:
time: 146 us
  Pallas kernels  144 us (99%)
  local copies, waits for them, and re-layouts  1.77 us (1%)
    pallas_call x1, Pallas kernels, shards(): pl.pallas_call(functools.partial(kernel, sizes), out_shape=jax.ShapeDtype...  144 us

profile of v4, /device:TPU:33, one launch (start us, length us, event | category | flops | bytes accessed | tf_op | source)
XLA Modules:
  0.0 146.2 jit_solution(12899980055883306431)
XLA Ops:
  0.0 144.4 %layers.1 = bf16[384,512]{1,0:T(8,128)(2,1)} custom-call(bf16[384,512]{1,0:T(8,128)(2,1)} %hidden.1, f32[2,512]{1,0:T(2,128)} %in_gain_in.1, bf16[2,256,256]{2,1,0:T(8,128)(2,1)} %w_value.1, bf16[2,256,256]{2,1,0:T(8,128)(2,1)} %w_gate.1, f32[31,2,256]{2,1,0:T(2,128)} %bitcast.1, f32[2,256]{1,0:T(2,128)} %norm_gain_in.1, f32[2,256]{1,0:T(2,128)} %norm_shift_in.1, ...), custom_call_target="tpu_custom_call" | custom-call | tf_op jit(solution)/shard_map/layers/pallas_call | solution.py:717
  144.4 1.8 %copy.10 = bf16[384,512]{1,0:T(8,128)(2,1)} copy(bf16[384,512]{1,0:T(8,128)(2,1)} %layers.1) | data formatting | bytes 786432

commit v5 on v4

--- a/solution.py
+++ b/solution.py
@@ -101,13 +101,16 @@
         y = lax.axis_index("grp")
         par = lax.rem(y, 2)
         y_mate = y + 1 - 2 * par
-        lone = 80
-        ring_rows = rows_w - lone
-        ring_base = par * lone
-        y_out_at = pl.ds(pl.multiple_of(par * ring_rows, 16), lone)
-        y_in_at = pl.ds(pl.multiple_of((1 - par) * ring_rows, 16), lone)
+        lone = (96, 80, 80)
     else:
-        ring_rows, ring_base = rows_w, 0
+        par, lone = 0, (0, 0, 0)
+    ring_rows = tuple(rows_w - rows for rows in lone)
+
+    def rows_at(offset, rows):
+        return pl.ds(pl.multiple_of(offset, 16), rows)
+
+    def lone_at(sub):
+        return rows_at(par * ring_rows[sub], lone[sub])
 
     def zc(offset):
         return lax.rem(z + offset + 2 * ns, ns)
@@ -117,7 +120,9 @@
             src_ref=src, dst_ref=dst, send_sem=ssem, recv_sem=rsem, device_id=where, device_id_type=MESH
         )
 
-    early, late = (0, 1), (2,)
+    split = 96
+    pieces = ((0, 0, ring_rows[0]), (1, 0, ring_rows[1]), (2, 0, split), (2, split, ring_rows[2] - split))
+    early, late = (0, 1), (2, 3)
     first_core = c == 0
     second_core = c == 1
 
@@ -125,7 +130,8 @@
         return remote(wbuf.at[l, 0, z], wbuf.at[l, 1, z], m_send.at[l], m_recv.at[l], tp=t_mate)
 
     def ring_part(l, col, chunk, sub):
-        return wbuf.at[l, col, chunk, sub, pl.ds(pl.multiple_of(ring_base, 16), ring_rows), :]
+        matrix, at, rows = pieces[sub]
+        return wbuf.at[l, col, chunk, matrix, rows_at(par * lone[matrix] + at, rows), :]
 
     def z_copy(l, col, sub, d, s):
         at, way = ring_part(l, col, zc(-d * (s - 1)), sub), 0 if d == RIGHT else 1
@@ -138,7 +144,7 @@
     def active(l, sub, d, s):
         if s < half:
             return True
-        return s == half and d == (RIGHT, LEFT, RIGHT if l % 2 == 0 else LEFT)[sub]
+        return s == half and d == (RIGHT, LEFT, RIGHT, LEFT)[sub]
 
     bulk = half - 2
 
@@ -154,12 +160,11 @@
         src, dst = ring_part(l, 1, chunk, sub), ring_part(l, 0, chunk, sub)
         return remote(src, dst, g_send.at[l], w_recv.at[l, place(kind, d, s)], tp=t_mate)
 
-    def y_copy(l, col, kind, d, s, rows):
-        chunk = zc(-d * s)
-        subs = pl.ds(0, 2) if kind == 0 else pl.ds(2, 1)
-        src, dst = wbuf.at[l, col, chunk, subs, rows, :], wbuf.at[l, 0, chunk, subs, rows, :]
+    def y_copy(l, col, matrix, d, s):
+        chunk, rows = zc(-d * s), lone_at(matrix)
+        src, dst = wbuf.at[l, col, chunk, matrix, rows, :], wbuf.at[l, 0, chunk, matrix, rows, :]
         where = {"grp": y_mate} if col == 0 else {"grp": y_mate, "tp": t_mate}
-        return remote(src, dst, y_send.at[l], w_recv.at[l, place(kind, d, s)], **where)
+        return remote(src, dst, y_send.at[l], w_recv.at[l, place(matrix // 2, d, s)], **where)
 
     def hop_ways(s):
         return (RIGHT, LEFT) if 0 < s < half else (RIGHT,)
@@ -180,7 +185,7 @@
     def serve(l, kind, s, some=None):
         subs = (early, late)[kind]
         for sub in some or subs:
-            for col in (1, 0):
+            for col in (0, 1) if l == 0 and s == 1 else (1, 0):
                 for d in (RIGHT, LEFT):
                     if not active(l, sub, d, s):
                         continue
@@ -189,21 +194,20 @@
                         z_copy(l, col, sub, d, s + 1).start()
                     if col == 1:
                         give_mate(l, kind, sub, d, s).start()
-                    if paired and sub == subs[-1]:
-                        y_copy(l, col, kind, d, s, y_out_at).start()
-
-    def take(l, kind, s, rows):
-        if s == 0:
+                    if paired and sub != late[0]:
+                        y_copy(l, col, pieces[sub][0], d, s).start()
+
+    def take(l, kind, s, matrices, rows):
+        if s == 0 or (kind == 0 and s < bulk):
             return
         if kind == 1:
-            parts = [(wbuf.at[l, 0, pl.ds(0, ns - 1), 2, pl.ds(0, rows), :], 4)]
-        elif s < bulk:
-            return
+            parts = [(ns - 1, 4)]
         elif s == bulk:
-            parts = [(wbuf.at[l, 0, pl.ds(0, 2 * bulk), pl.ds(0, 2), pl.ds(0, rows), :], 0)]
+            parts = [(2 * bulk, 0)]
         else:
-            parts = [(wbuf.at[l, 0, 0, pl.ds(0, 2), pl.ds(0, rows), :], place(0, d, s)) for d in hop_ways(s)]
-        for part, sem in parts:
+            parts = [(1, place(0, d, s)) for d in hop_ways(s)]
+        for chunks, sem in parts:
+            part = wbuf.at[l, 0, pl.ds(0, chunks), pl.ds(0, matrices), pl.ds(0, rows), :]
             pltpu.make_async_copy(part, part, w_recv.at[l, sem]).wait()
 
     def w_wait(l, kind, s):
@@ -211,11 +215,11 @@
 
             @pl.when(second_core)
             def _():
-                take(l, kind, s, lone)
+                take(l, kind, s, 1, lone[2] if kind else lone[0] + lone[1])
 
         @pl.when(first_core)
         def _():
-            take(l, kind, s, rows_w)
+            take(l, kind, s, 2 - kind, rows_w)
 
     def w_drain(l):
         def wait(part, sem):
@@ -223,11 +227,16 @@
 
         @pl.when(second_core)
         def _():
-            sent = wbuf.at[l, :, pl.ds(0, ns - 1), :, pl.ds(0, ring_rows), :]
+            def total(rows):
+                subs, rest = rows // rows_w, rows % rows_w
+                assert rest == 0
+                return wbuf.at[l, :, pl.ds(0, ns - 1), pl.ds(0, subs), :, :]
+
+            sent = total(sum(ring_rows))
             wait(sent, z_send.at[l])
             wait(sent.at[0], g_send.at[l])
             if paired:
-                wait(wbuf.at[l, :, pl.ds(0, ns - 1), :, pl.ds(0, lone), :], y_send.at[l])
+                wait(total(sum(lone)), y_send.at[l])
 
         @pl.when(first_core)
         def _():
@@ -637,9 +646,8 @@
             def _():
                 x_end(n)
 
-            for s in range(7):
+            for s in range(half):
                 ring_mm(n, s)
-            ring_mm(n, half - 1)
             steps(n, half + 1, half + 2)
             ring_mm(n, half)
 
@@ -696,7 +704,7 @@
             dma((layers + 5,)),
             dma((2,)),
             dma((layers,)),
-            dma((2, 3, 2, 4)),
+            dma((2, 4, 2, 4)),
             dma((layers,)),
             dma((layers,)),
             dma((layers, 5)),

time: 146 us -> 144 us (0.986)
  Pallas kernels: 144 us -> 142 us
    pallas_call x1, Pallas kernels: 144 us -> 142 us  [shards(): pl.pallas_call(functools.partial(kernel, sizes), out_shape=jax.ShapeDtype...]
where the time goes in v5:
time: 144 us
  Pallas kernels  142 us (99%)
  local copies, waits for them, and re-layouts  1.77 us (1%)
    pallas_call x1, Pallas kernels, shards(): pl.pallas_call(functools.partial(kernel, sizes), out_shape=jax.ShapeDtype...  142 us

profile of v5, /device:TPU:33, one launch (start us, length us, event | category | flops | bytes accessed | tf_op | source)
XLA Modules:
  0.0 143.5 jit_solution(11338911074271377515)
XLA Ops:
  0.0 141.7 %layers.1 = bf16[384,512]{1,0:T(8,128)(2,1)} custom-call(bf16[384,512]{1,0:T(8,128)(2,1)} %hidden.1, f32[2,512]{1,0:T(2,128)} %in_gain_in.1, bf16[2,256,256]{2,1,0:T(8,128)(2,1)} %w_value.1, bf16[2,256,256]{2,1,0:T(8,128)(2,1)} %w_gate.1, f32[31,2,256]{2,1,0:T(2,128)} %bitcast.1, f32[2,256]{1,0:T(2,128)} %norm_gain_in.1, f32[2,256]{1,0:T(2,128)} %norm_shift_in.1, ...), custom_call_target="tpu_custom_call" | custom-call | tf_op jit(solution)/shard_map/layers/pallas_call | solution.py:725
  141.8 1.8 %copy.10 = bf16[384,512]{1,0:T(8,128)(2,1)} copy(bf16[384,512]{1,0:T(8,128)(2,1)} %layers.1) | data formatting | bytes 786432

commit v6 on v5

--- a/solution.py
+++ b/solution.py
@@ -380,13 +380,11 @@
         halo_out[l] = ext[tokens : tokens + reach, :].astype(BF16)
         halo_copy(l).start()
 
-    small = 32
-
-    def conv_rows(l, lo, hi):
+    def conv_rows(l, base, small, count):
         offset = reach - (n_taps - 1)
 
         def step(i, carry):
-            at = pl.multiple_of(i * small, small)
+            at = pl.multiple_of(base + i * small, 8)
             total = jnp.zeros((small, ch), F32)
             for k in range(n_taps):
                 a, b = ((k + offset) // 8) * 8, (k + offset) % 8
@@ -396,13 +394,13 @@
             conved[pl.ds(at, small), :] = total
             return carry
 
-        lax.fori_loop(lo, hi, step, 0)
+        lax.fori_loop(0, count, step, 0)
 
     def conv_body(l):
         span = shifted.shape[1]
         for b in range(1, 8):
             shifted[b - 1, reach:, :] = ext[reach + b : span + b, :]
-        conv_rows(l, 1, tokens // small)
+        conv_rows(l, reach, 88, (tokens - reach) // 88)
 
     def conv_head(l):
         halo_copy(l).wait_recv()
@@ -410,7 +408,7 @@
         ext[:reach, :] = jnp.where(z > 0, before, jnp.zeros_like(before))
         for b in range(1, 8):
             shifted[b - 1, :reach, :] = ext[b : reach + b, :]
-        conv_rows(l, 0, 1)
+        conv_rows(l, 0, reach, 1)
         value = conved[...]
         sums = jnp.sum(value, axis=1, keepdims=True)
         spread = value - sums / ch
@@ -465,10 +463,13 @@
         c_out[l, slot] = total.astype(BF16)
         c_copy(l, slot).start()
 
-    def settle(l, h, last):
+    def own_part(l, h):
         total = project(l, 0, c, h)
         p_copy(l, h).wait_recv()
-        total = total + p_in[l, h].astype(F32)
+        (acc_v, acc_g)[h][...] = total + p_in[l, h].astype(F32)
+
+    def settle(l, h, last):
+        total = (acc_v, acc_g)[h][...]
         for slot in (2 + h, 4 + h):
             c_copy(l, slot).wait_recv()
             total = total + c_in[l, slot].astype(F32)
@@ -629,6 +630,8 @@
         part(3, 1)
         if not final:
             z_first(n, late)
+        own_part(l, 0)
+        own_part(l, 1)
         more(4)
         settle(l, 0, final)
         settle(l, 1, final)
@@ -721,18 +724,20 @@
             dma((layers,)),
             dma((6,)),
         ]
-        a = pl.BlockSpec(memory_space=pl.ANY)
+        a, b = pl.BlockSpec(memory_space=pltpu.HBM), pl.BlockSpec(memory_space=pl.ANY)
+        taps = jnp.transpose(conv_taps, (1, 0, 2))
+        operands = (hidden_in, in_gain, w_value, w_gate, taps, norm_gain, norm_shift, w_out)
         return pl.pallas_call(
             functools.partial(kernel, sizes),
             out_shape=jax.ShapeDtypeStruct(hidden_in.shape, hidden_in.dtype),
             in_specs=[a] * 8,
-            out_specs=a,
+            out_specs=b,
             scratch_shapes=scratch,
             name="layers",
             compiler_params=pltpu.CompilerParams(
-                collective_id=0, has_side_effects=True, vmem_limit_bytes=60 * 2**20
+                collective_id=0, has_side_effects=True, vmem_limit_bytes=52 * 2**20
             ),
-        )(hidden_in, in_gain, w_value, w_gate, jnp.transpose(conv_taps, (1, 0, 2)), norm_gain, norm_shift, w_out)
+        )(*(pltpu.with_memory_space_constraint(operand, pltpu.HBM) for operand in operands))
 
     placed = (
         P(("grp", "sp"), "tp"),

time: 144 us -> 141 us (0.979)
  no operation moved by 1% of the time
where the time goes in v6:
time: 141 us
  Pallas kernels  141 us (100%)
    pallas_call x1, Pallas kernels, shards(): pl.pallas_call(functools.partial(kernel, sizes), out_shape=jax.ShapeDtype...  141 us

profile of v6, /device:TPU:33, one launch (start us, length us, event | category | flops | bytes accessed | tf_op | source)
XLA Modules:
  0.0 141.3 jit_solution(7418017482375437625)
XLA Ops:
  0.0 140.6 %layers.1 = bf16[384,512]{1,0:T(8,128)(2,1)S(1)} custom-call(bf16[384,512]{1,0:T(8,128)(2,1)} %hidden.1, f32[2,512]{1,0:T(2,128)} %in_gain_in.1, bf16[2,256,256]{2,1,0:T(8,128)(2,1)} %w_value.1, bf16[2,256,256]{2,1,0:T(8,128)(2,1)} %w_gate.1, f32[31,2,256]{2,1,0:T(2,128)} %bitcast.1, f32[2,256]{1,0:T(2,128)} %norm_gain_in.1, f32[2,256]{1,0:T(2,128)} %norm_shift_in.1, ...), custom_call_target="tpu_custom_call" | custom-call | tf_op jit(solution)/shard_map/layers/pallas_call | solution.py:730
  140.6 0.7 copy.10
